TPU v7x, 32 devices: a whole 2x2x4 slice. The times are simulated.
32 devices in a mesh: kv: 8 (over z, y), tp: 4 (over x, core).
Axes of the slice: x: 2, y: 2, z: 4, core: 2. Of those that a mesh axis runs over, the one named last changes fastest.
Arguments:
- tokens: bfloat16 [256, 4, 2048], P(None, None, ('kv', 'tp')), may hold values from -520 to 520
- input_norm_gain: bfloat16 [2048], replicated, may hold values from 0.099609375 to 1.8984375
- query_weight: bfloat16 [2048, 2048], P(None, 'kv'), may hold values from -0.125 to 0.125
- key_weight: bfloat16 [2048, 2048], P(None, 'kv'), may hold values from -0.125 to 0.125
- value_weight: bfloat16 [2048, 16, 128], P(None, 'kv', 'tp'), may hold values from -1.14904852 to 1.14904852
- output_gate_weight: bfloat16 [2048, 16, 128], P(None, 'kv', 'tp'), may hold values from -0.125 to 0.125
- strength_weight: bfloat16 [2048, 16], P(None, 'kv'), may hold values from -0.125 to 0.125
- decay_weight: bfloat16 [2048, 16], P(None, 'kv'), may hold values from -0.125 to 0.125
- head_decay_rate: float32 [16], P('kv'), may hold values from 0.005 to 1.5
- proposal_log_decay: float32 [256, 4, 16], P(None, None, 'kv'), may hold values from -0.69 to 0
- head_norm_gain: bfloat16 [128], P('tp'), may hold values from 0.099609375 to 1.8984375
- output_weight: bfloat16 [16, 128, 2048], P('kv', 'tp'), may hold values from -1.14904852 to 1.14904852
- output_norm_gain: bfloat16 [2048], P(('kv', 'tp')), may hold values from 0.099609375 to 1.8984375
- state: float32 [256, 16, 128, 128], P(None, 'kv', 'tp'), may hold values from -4.5961941 to 4.5961941
- previous_keys: bfloat16 [256, 4, 2048], P(None, None, 'kv'), may hold values from -6 to 6
- previous_values: bfloat16 [256, 4, 16, 128], P(None, None, 'kv', 'tp'), may hold values from -52 to 52
- previous_log_decay: float32 [256, 4, 16], P(None, None, 'kv'), may hold values from -0.7 to -0.02
- previous_strengths: float32 [256, 4, 16], P(None, None, 'kv'), may hold values from 0.1 to 0.9
- accepted: int32 [256], replicated, may hold values from 0 to 4
- parent: int32 [256, 4], replicated, may hold values from -1 to 2, as said below
Outputs:
- layer_out: bfloat16 [256, 4, 2048], P(None, None, ('kv', 'tp'))
- accepted_state: float32 [256, 16, 128, 128], P(None, 'kv', 'tp')
Inputs may be any that keep to these rules, and one draw needn't show every extreme that they name: parent[b, i] is -1 or a proposal index below i; -1 means that proposal i follows the accepted old proposals directly.
All inputs are finite; a program needn't handle non-finite values.
Results may differ from a plain program's by a relative error of at most 0.019.
Values may be sent and summed in bfloat16 or wider, within the bound.
A program may use at most 128 MiB of HBM per device.

v0:
```python
import functools

import jax
import jax.numpy as jnp
from jax import lax
from jax.experimental import pallas as pl
from jax.experimental.pallas import tpu as pltpu
from jax.sharding import PartitionSpec as P

epsilon = 1e-06
GROUP = 16
AXES = ("kv", "tp")


def total(terms):
    terms = list(terms)
    while len(terms) > 1:
        terms = [sum(terms[i : i + 2][1:], terms[i]) for i in range(0, len(terms), 2)]
    return terms[0]


def delta_kernel(
    prop, q_ref, k_ref, ok_ref, v_ref, ov_ref, sc_ref, s_ref, o_ref, sq_ref, out_ref, kt_ref, eg_ref
):
    lanes = s_ref.shape[0]
    vdim = s_ref.shape[2]
    hd = s_ref.shape[3]
    groups = lanes // GROUP
    f32, bf16 = jnp.float32, jnp.bfloat16

    for index, ref in enumerate((ok_ref, k_ref, q_ref)):
        for p in range(prop):
            tile = ref[p * lanes : (p + 1) * lanes, :].astype(f32)
            kt_ref[index * prop + p] = tile.T
    positions = 2 * prop
    square = [jnp.sum(kt_ref[i] * kt_ref[i], axis=0, keepdims=True) for i in range(3 * prop)]
    inv = [lax.rsqrt(x + epsilon) for x in square]
    inv = inv[:positions] + [x * hd ** (-0.5) for x in inv[positions:]]

    def scalar(row, p):
        return sc_ref[0, row : row + 1, p * lanes : (p + 1) * lanes]

    beta = [scalar(0, p) for p in range(prop)] + [scalar(2, p) for p in range(prop)]
    g = [scalar(1, p) for p in range(prop)] + [scalar(3, p) for p in range(prop)]
    parents = [scalar(4, p) for p in range(prop)]
    ancestor = []
    for i in range(prop):
        direct = [jnp.where(parents[i] == float(j), 1.0, 0.0) for j in range(i)]
        row = []
        for j in range(i):
            row.append(total([direct[j]] + [direct[m] * ancestor[m][j] for m in range(j + 1, i)]))
        ancestor.append(row)

    def vis(i, j):
        if i < prop or j < prop:
            return None
        return ancestor[i - prop][j - prop]

    gam = []
    for i in range(positions):
        acc = g[i]
        for j in range(i):
            seen = vis(i, j)
            acc = acc + (g[j] if seen is None else seen * g[j])
        gam.append(acc)
    eg = [jnp.exp(x) for x in gam]

    def decay(i, j):
        value = jnp.exp(jnp.minimum(gam[i] - gam[j], 0.0))
        seen = vis(i, j)
        return value if seen is None else value * seen

    def gram(i, j):
        return jnp.sum(kt_ref[i] * kt_ref[j], axis=0, keepdims=True) * (inv[i] * inv[j])

    dec = {(i, j): decay(i, j) for i in range(positions) for j in range(i)}
    coupling = {(i, j): beta[i] * gram(i, j) * dec[i, j] for (i, j) in dec}
    reach = {}
    for p in range(prop):
        i = prop + p
        for j in range(i + 1):
            value = gram(positions + p, j)
            reach[p, j] = value if j == i else value * dec[i, j]

    last = eg[prop - 1]
    eg_ref[...] = jnp.broadcast_to(last, (lanes, lanes)).T

    lane = lax.broadcasted_iota(jnp.int32, (vdim, lanes), 1)
    inner, outer = lane % GROUP, lane // GROUP
    products = []
    for c in range(groups):
        rows = s_ref[c * GROUP : (c + 1) * GROUP, 0].reshape(GROUP * vdim, hd).astype(bf16)
        tiles = []
        for ref in (ok_ref, k_ref, q_ref):
            for p in range(prop):
                start = p * lanes + c * GROUP
                tiles.append(ref[start : start + GROUP, :])
        keys = jnp.concatenate(tiles, axis=0)
        product = lax.dot_general(
            rows, keys, (((1,), (1,)), ((), ())), preferred_element_type=f32
        )
        wide = []
        for first in range(0, 3 * prop * GROUP, lanes):
            width = min(lanes, 3 * prop * GROUP - first)
            part = product[:, first : first + width]
            chosen = part[:vdim]
            for s in range(1, GROUP):
                mask = (inner if width == lanes else inner[:, :width]) == s
                chosen = jnp.where(mask, part[s * vdim : (s + 1) * vdim], chosen)
            if width < lanes:
                chosen = jnp.concatenate(
                    [chosen, jnp.zeros((vdim, lanes - width), f32)], axis=1
                )
            wide.append(chosen)
        products.append(wide)

    per_tile = lanes // GROUP

    def swap(source, sources, targets):
        shifted = []
        for d in range(groups):
            acc = None
            for a in range(sources):
                t = (a - d) % groups
                if t >= targets:
                    continue
                acc = source[a] if acc is None else jnp.where(outer == t, source[a], acc)
            shifted.append(acc if acc is None or d == 0 else pltpu.roll(acc, d * GROUP, 1))
        results = []
        for t in range(targets):
            acc = None
            for a in range(sources):
                piece = shifted[(a - t) % groups]
                acc = piece if acc is None else jnp.where(outer == a, piece, acc)
            results.append(acc)
        return results

    raw = []
    for tile in range(len(products[0])):
        count = min(per_tile, 3 * prop - tile * per_tile)
        raw += swap([products[c][tile] for c in range(groups)], groups, count)

    update = []
    for i in range(positions):
        source = ov_ref if i < prop else v_ref
        p = i % prop
        value = source[:, p * lanes : (p + 1) * lanes].astype(f32)
        acc = beta[i] * value - (beta[i] * eg[i] * inv[i]) * raw[i]
        for j in range(i):
            acc = acc - coupling[i, j] * update[j]
        update.append(acc)

    for p in range(prop):
        i = prop + p
        acc = (eg[i] * inv[positions + p]) * raw[positions + p]
        for j in range(i + 1):
            acc = acc + reach[p, j] * update[j]
        o_ref[0, :, p * lanes : (p + 1) * lanes] = acc
        sq_ref[0, :, p * lanes : (p + 1) * lanes] = jnp.sum(acc * acc, axis=0, keepdims=True)

    weighted = [
        update[j] * (jnp.exp(gam[prop - 1] - gam[j]) * inv[j]) for j in range(prop)
    ]
    compact = swap(weighted, prop, groups)
    width = prop * GROUP
    narrow = inner[:, :width]
    for c in range(groups):
        tiles = [
            ok_ref[p * lanes + c * GROUP : p * lanes + (c + 1) * GROUP, :] for p in range(prop)
        ]
        keys = jnp.concatenate(tiles, axis=0)
        piece = compact[c][:, :width]
        left = jnp.concatenate(
            [jnp.where(narrow == s, piece, 0.0) for s in range(GROUP)], axis=0
        ).astype(bf16)
        delta = jnp.dot(left, keys, preferred_element_type=f32)
        for s in range(GROUP):
            seq = c * GROUP + s
            out_ref[seq, 0] = (
                s_ref[seq, 0] * eg_ref[seq : seq + 1, :hd] + delta[s * vdim : (s + 1) * vdim]
            )


def delta_call(prop, lanes, q, k, ok, v, ov, scal, state):
    seqs, heads, vdim, hd = state.shape
    tiles = seqs // lanes
    block = prop * lanes
    natural = pl.BlockSpec((block, hd), lambda t, h: (t, h))
    turned = pl.BlockSpec((vdim, block), lambda t, h: (h, t))
    state_spec = pl.BlockSpec((lanes, 1, vdim, hd), lambda t, h: (t, h, 0, 0))
    return pl.pallas_call(
        functools.partial(delta_kernel, prop),
        grid=(tiles, heads),
        in_specs=[
            natural,
            natural,
            natural,
            turned,
            turned,
            pl.BlockSpec((1, 8, block), lambda t, h: (h, 0, t)),
            state_spec,
        ],
        out_specs=[
            pl.BlockSpec((1, vdim, block), lambda t, h: (h, 0, t)),
            pl.BlockSpec((1, 1, block), lambda t, h: (h, 0, t)),
            state_spec,
        ],
        out_shape=[
            jax.ShapeDtypeStruct((heads, vdim, seqs * prop), jnp.float32),
            jax.ShapeDtypeStruct((heads, 1, seqs * prop), jnp.float32),
            jax.ShapeDtypeStruct(state.shape, jnp.float32),
        ],
        scratch_shapes=[
            pltpu.VMEM((3 * prop, hd, lanes), jnp.float32),
            pltpu.VMEM((lanes, lanes), jnp.float32),
        ],
        compiler_params=pltpu.CompilerParams(vmem_limit_bytes=40 * 1024 * 1024),
        cost_estimate=pl.CostEstimate(
            flops=2 * seqs * heads * vdim * hd * 256,
            bytes_accessed=8 * seqs * heads * vdim * hd,
            transcendentals=0,
        ),
    )(q, k, ok, v, ov, scal, state)


def scattered_sum(blended, weight, own):
    f32, bf16 = jnp.float32, jnp.bfloat16
    channels, rows = blended.shape
    kv, tp = lax.axis_size("kv"), lax.axis_size("tp")
    chips = tp // 2
    core = lax.axis_index("tp") % 2
    halves = weight.reshape(channels, kv * chips, 2, own)

    def half(which):
        part = lax.dynamic_index_in_dim(halves, which, 2, keepdims=False)
        return lax.dot_general(
            part.reshape(channels, kv * chips * own),
            blended,
            (((0,), (0,)), ((), ())),
            preferred_element_type=f32,
        )

    pairs = [(i, i ^ 1) for i in range(tp)]
    received = lax.ppermute(half(1 - core).astype(bf16), "tp", pairs)
    summed = (half(core) + received.astype(f32)).astype(bf16).reshape(kv, chips, own, rows)
    if chips == 2:
        x = lax.axis_index("tp") // 2
        across = [(i, i ^ 2) for i in range(tp)]
        other = lax.dynamic_index_in_dim(summed, 1 - x, 1, keepdims=False)
        mine = lax.dynamic_index_in_dim(summed, x, 1, keepdims=False)
        other = lax.ppermute(other, "tp", across)
        summed = (mine.astype(f32) + other.astype(f32)).astype(bf16)
    else:
        groups = [[2 * x + c for x in range(chips)] for c in range(2)]
        parts = lax.all_to_all(summed, "tp", 1, 1, axis_index_groups=groups, tiled=True)
        summed = jnp.sum(parts.astype(f32), axis=1).astype(bf16)
    parts = lax.all_to_all(summed, "kv", 0, 0, tiled=True)
    return jnp.sum(parts.astype(f32), axis=0)


def on_device(
    tokens,
    input_norm_gain,
    query_weight,
    key_weight,
    value_weight,
    output_gate_weight,
    strength_weight,
    decay_weight,
    head_decay_rate,
    proposal_log_decay,
    head_norm_gain,
    output_weight,
    output_norm_gain,
    state,
    previous_keys,
    previous_values,
    previous_log_decay,
    previous_strengths,
    accepted,
    parent,
):
    f32, bf16 = jnp.float32, jnp.bfloat16
    seqs, heads, vdim, hd = state.shape
    prop = parent.shape[1]
    rows = seqs * prop
    width = input_norm_gain.shape[0]
    lanes = min(128, seqs)
    tiles = seqs // lanes

    def order(x):
        tail = x.shape[2:]
        x = x.reshape((tiles, lanes, prop) + tail)
        return x.swapaxes(1, 2).reshape((rows,) + tail)

    own = tokens.shape[2]
    gathered = lax.all_gather(order(tokens), AXES, axis=1, tiled=True)
    features = gathered.astype(f32)
    normed = features * lax.rsqrt(jnp.mean(features * features, axis=-1, keepdims=True) + epsilon)
    normed = (normed * input_norm_gain.astype(f32)).astype(bf16)

    queries = jnp.dot(normed, query_weight, preferred_element_type=f32).astype(bf16)
    keys = jnp.dot(normed, key_weight, preferred_element_type=f32).astype(bf16)
    small = jnp.concatenate(
        [
            value_weight.reshape(width, -1),
            output_gate_weight.reshape(width, -1),
            strength_weight,
            decay_weight,
        ],
        axis=1,
    )
    side = lax.dot_general(
        small, normed, (((0,), (1,)), ((), ())), preferred_element_type=f32
    )
    channels = heads * vdim
    values = side[:channels].astype(bf16)
    zgate = side[channels : 2 * channels].astype(bf16).astype(f32)
    strength = side[2 * channels : 2 * channels + heads]
    decay_pre = side[2 * channels + heads :]

    beta_new = jax.nn.sigmoid(strength)
    g_new = -head_decay_rate[:, None] * jax.nn.softplus(decay_pre) + order(proposal_log_decay).T
    position = jnp.arange(prop, dtype=jnp.int32)
    live = (position[None, :] < accepted[:, None]).astype(f32)[:, :, None]
    beta_old = order(previous_strengths * live).T
    g_old = order(previous_log_decay * live).T
    parents = jnp.broadcast_to(order(parent).astype(f32)[None], (heads, rows))
    zero = jnp.zeros((heads, rows), f32)
    scal = jnp.stack([beta_old, g_old, beta_new, g_new, parents, zero, zero, zero], axis=1)
    old_keys = order(previous_keys)
    old_values = order(previous_values).reshape(rows, channels).T

    readout, squares, accepted_state = delta_call(
        prop, lanes, queries, keys, old_keys, values, old_values, scal, state
    )
    squares = lax.psum(squares.reshape(heads, rows), "tp")
    scale = lax.rsqrt(squares / hd + epsilon)[:, None, :]
    blended = readout * scale * head_norm_gain.astype(f32)[None, :, None]
    blended = blended * jax.nn.silu(zgate).reshape(heads, vdim, rows)
    blended = blended.reshape(channels, rows).astype(bf16)
    share = scattered_sum(blended, output_weight.reshape(channels, width), own)
    sumsq = lax.psum(jnp.sum(share * share, axis=0), AXES)
    scaling = lax.rsqrt(sumsq / width + epsilon)[None, :]
    layer_out = (share * scaling * output_norm_gain.astype(f32)[:, None]).astype(bf16).T
    layer_out = layer_out.reshape(tiles, prop, lanes, own).swapaxes(1, 2)
    return (layer_out.reshape(seqs, prop, own), accepted_state)


def solution(mesh):
    placed = (
        P(None, None, AXES),
        P(),
        P(None, "kv"),
        P(None, "kv"),
        P(None, "kv", "tp"),
        P(None, "kv", "tp"),
        P(None, "kv"),
        P(None, "kv"),
        P("kv"),
        P(None, None, "kv"),
        P("tp"),
        P("kv", "tp", None),
        P(AXES),
        P(None, "kv", "tp", None),
        P(None, None, "kv"),
        P(None, None, "kv", "tp"),
        P(None, None, "kv"),
        P(None, None, "kv"),
        P(),
        P(),
    )
    return jax.shard_map(
        on_device,
        mesh=mesh,
        in_specs=placed,
        out_specs=(P(None, None, AXES), P(None, "kv", "tp", None)),
        check_vma=False,
    )
```

profile of v0, /device:TPU:0, one launch (start us, length us, event | category | flops | bytes accessed | tf_op | source)
XLA Modules:
  0.0 216.4 jit_solution(10820136725009665674)
XLA Ops:
  7.2 1.1 reshape.113
  8.5 0.7 reshape.114
  9.3 0.7 neg.16
  9.9 0.7 convert_element_type.93
  10.6 0.7 convert_element_type.89
  11.3 0.7 convert_element_type.84
  11.9 0.7 reshape.124
  12.7 0.7 fusion.21
  13.4 0.7 broadcast_multiply_fusion
  14.2 0.9 reshape.119
  15.5 1.5 reshape_reshape.6
  17.0 3.5 %dynamic-slice_reduce_fusion = (bf16[64,16,64]{2,1,0:T(8,128)(2,1)S(1)}, bf16[64,16,64]{2,1,0:T(8,128)(2,1)S(1)}) fusion(bf16[64,16,2,64]{3,2,1,0:T(2,128)(2,1)S(1)} %reshape_reshape.6, s32[]{:T(128)S(6)} %select_n.32, s32[]{:T(128)S(6)} %select_n.30), kind=kLoop, calls=%fused_computation.21 | loop fusion | bytes 524296 | tf_op jit(solution)/shard_map/jit(dynamic_index_in_dim)/dynamic_slice | solution.py:235
  20.5 0.9 reshape.128
  21.4 54.5 %all-gather.2.cloned.1.call-done = bf16[1024,2048]{0,1:T(8,128)(2,1)} async-done(((bf16[1024,64]{0,1:T(8,128)(2,1)}), bf16[1024,2048]{0,1:T(8,128)(2,1)}) %all-gather.2.cloned.1.call-update) | async-done | bytes 4194320 | tf_op jit(solution)/shard_map/all_gather | solution.py:297
  75.9 3.3 %fusion = f32[1024]{0:T(1024)S(1)} fusion(bf16[1024,2048]{0,1:T(8,128)(2,1)} %all-gather.2.cloned.1.call-done), kind=kLoop, calls=%fused_computation.2 | loop fusion | flops 6290432 | bytes 4198400 | tf_op jit(solution)/shard_map/reduce_sum | solution.py:299
  79.4 1.4 fusion.26
  81.2 4.1 %convolution_convert_fusion.1.k_ref = bf16[1024,256]{1,0:T(8,128)(2,1)S(1)} fusion(bf16[2048,256]{1,0:T(8,128)(2,1)S(1)} %copy-done, bf16[1024,2048]{0,1:T(8,128)(2,1)} %all-gather.2.cloned.1.call-done, f32[2048]{0:T(1024)S(1)} %convert_element_type.84, f32[1024]{0:T(1024)S(1)} %add_rsqrt_fusion.2), kind=kOutput, calls=%fused_computation.10 | convolution fusion | flops 1082392576 | bytes 5779456 | tf_op jit(solution)/shard_map/dot_general | solution.py:303
  85.3 1.8 convolution_convert_fusion.2.q_ref
  87.7 9.3 %shard_map.203 = (f32[2,32,1024]{2,1,0:T(8,128)S(1)}, f32[2,1,1024]{2,1,0:T(1,128)S(1)}, f32[256,2,32,128]{3,2,1,0:T(8,128)}) custom-call(bf16[1024,256]{1,0:T(8,128)(2,1)S(1)} %convolution_convert_fusion.2.q_ref, bf16[1024,256]{1,0:T(8,128)(2,1)S(1)} %convolution_convert_fusion.1.k_ref, bf16[1024,256]{1,0:T(8,128)(2,1)S(1)} %bitcast.79, ...), custom_call_target="tpu_custom_call" | custom-call | flops 1073741824 | bytes 16777216 | tf_op jit(solution)/shard_map/pallas_call | solution.py:191
  97.0 6.9 %psum.14 = f32[2,1024]{1,0:T(2,128)S(1)} all-reduce(f32[2,1024]{1,0:T(2,128)S(1)} %bitcast.95), channel_id=1, replica_groups=mesh['kv'=8,'tp'=4] {'tp'}, use_global_device_ids=true, to_apply=%region_1.2 | all-reduce | flops 2048 | bytes 16384 | tf_op jit(solution)/shard_map/psum | solution.py:337
  104.0 1.6 convolution_convert_fusion
  105.7 0.9 reshape.112
  106.6 3.4 %collective-permute-done = bf16[1024,1024]{1,0:T(8,128)(2,1)} collective-permute-done((bf16[1024,1024]{1,0:T(8,128)(2,1)S(1)}, bf16[1024,1024]{1,0:T(8,128)(2,1)}, u32[]{:S(2)}, u32[]{:S(2)}) %collective-permute-start) | collective-permute-done | bytes 2097184 | tf_op jit(solution)/shard_map/ppermute | solution.py:244
  110.0 2.4 %add_convert_fusion = bf16[1024,1024]{1,0:T(8,128)(2,1)S(1)} fusion(bf16[1024,1024]{1,0:T(8,128)(2,1)} %collective-permute-done, bf16[64,1024]{1,0:T(8,128)(2,1)} %reshape.112, bf16[64,1024]{1,0:T(8,128)(2,1)S(1)} %bitcast.84), kind=kOutput, calls=%fused_computation.5 | convolution fusion | flops 137363456 | bytes 4456448 | tf_op jit(solution)/shard_map/dot_general | solution.py:236
  112.4 1.1 dynamic-slice_bitcast_fusion
  113.5 0.8 collective-permute-start.1
  114.3 24.7 %collective-permute-done.1 = bf16[8,64,1024]{2,1,0:T(8,128)(2,1)} collective-permute-done((bf16[8,64,1024]{2,1,0:T(8,128)(2,1)}, bf16[8,64,1024]{2,1,0:T(8,128)(2,1)}, u32[]{:S(2)}, u32[]{:S(2)}) %collective-permute-start.1) | collective-permute-done | bytes 1048608 | tf_op jit(solution)/shard_map/ppermute | solution.py:251
  139.1 2.6 %fusion.3 = bf16[8,64,1024]{2,1,0:T(8,128)(2,1)} fusion(bf16[8,64,1024]{2,1,0:T(8,128)(2,1)} %collective-permute-done.1, bf16[8,2,64,1024]{3,2,1,0:T(8,128)(2,1)S(1)} %bitcast.82, s32[]{:T(128)S(6)} %select_n.34), kind=kLoop, calls=%fused_computation.7 | loop fusion | flops 2097152 | bytes 3145732 | tf_op jit(solution)/shard_map/convert_element_type | solution.py:252
  141.7 3.6 %all-to-all-start = ((bf16[8,64,1024]{2,1,0:T(8,128)(2,1)}), bf16[8,64,1024]{2,1,0:T(8,128)(2,1)S(1)}, u32[]{:S(2)}, u32[]{:S(2)}) async-start(bf16[8,64,1024]{2,1,0:T(8,128)(2,1)} %fusion.3), calls=%async_computation | async-start | bytes 2097152 | tf_op jit(solution)/shard_map/all_to_all | solution.py:257
  145.3 25.5 %all-to-all-done = bf16[8,64,1024]{2,1,0:T(8,128)(2,1)S(1)} async-done(((bf16[8,64,1024]{2,1,0:T(8,128)(2,1)}), bf16[8,64,1024]{2,1,0:T(8,128)(2,1)S(1)}, u32[]{:S(2)}, u32[]{:S(2)}) %all-to-all-start) | async-done | bytes 1048608 | tf_op jit(solution)/shard_map/all_to_all | solution.py:257
  171.0 37.5 %psum.15 = f32[1024]{0:T(1024)S(1)} all-reduce(f32[1024]{0:T(1024)S(1)} %multiply_reduce_fusion), channel_id=1, replica_groups=mesh['kv'=8,'tp'=4] {'kv','tp'}, use_global_device_ids=true, to_apply=%region_4.5 | all-reduce | flops 1024 | bytes 8192 | tf_op jit(solution)/shard_map/psum | solution.py:343
  208.8 0.7 reshape.131
  (62 shorter events, 2.4 us)
Async XLA Ops:
  7.2 74.0 %copy-start = (bf16[2048,256]{1,0:T(8,128)(2,1)S(1)}, bf16[2048,256]{1,0:T(8,128)(2,1)}, u32[]{:S(2)}) copy-start(bf16[2048,256]{1,0:T(8,128)(2,1)} %param.23) | copy-start | bytes 3145732
  7.2 14.2 %copy-start.3 = (bf16[256,4,256]{2,1,0:T(4,128)(2,1)S(1)}, bf16[256,4,256]{2,1,0:T(4,128)(2,1)}, u32[]{:S(2)}) copy-start(bf16[256,4,256]{2,1,0:T(4,128)(2,1)} %param.34) | copy-start | bytes 1572868
  7.2 68.7 %all-gather.2.cloned.1.call-start = ((), (), s32[]{:S(2)}) async-start(), calls=%async_computation.1 | async-start | bytes 4325376 | tf_op jit(solution)/shard_map/all_gather | solution.py:297
  15.3 63.9 %copy-start.5 = (bf16[2048,2,32]{0,2,1:T(8,128)(2,1)S(1)}, bf16[2048,2,32]{0,2,1:T(8,128)(2,1)}, u32[]{:S(2)}) copy-start(bf16[2048,2,32]{0,2,1:T(8,128)(2,1)} %param.25) | copy-start | bytes 786436
  15.4 63.9 %copy-start.6 = (bf16[2048,2,32]{0,2,1:T(8,128)(2,1)S(1)}, bf16[2048,2,32]{0,2,1:T(8,128)(2,1)}, u32[]{:S(2)}) copy-start(bf16[2048,2,32]{0,2,1:T(8,128)(2,1)} %param.24) | copy-start | bytes 786436
  15.4 63.9 %copy-start.7 = (bf16[2048,2]{0,1:T(2,128)(2,1)S(1)}, bf16[2048,2]{0,1:T(2,128)(2,1)}, u32[]{:S(2)}) copy-start(bf16[2048,2]{0,1:T(2,128)(2,1)} %param.27) | copy-start | bytes 24580
  15.4 63.9 %copy-start.8 = (bf16[2048,2]{0,1:T(2,128)(2,1)S(1)}, bf16[2048,2]{0,1:T(2,128)(2,1)}, u32[]{:S(2)}) copy-start(bf16[2048,2]{0,1:T(2,128)(2,1)} %param.26) | copy-start | bytes 24580
  75.9 3.4 %copy-start.1 = (bf16[1024,2048]{0,1:T(8,128)(2,1)S(1)}, bf16[1024,2048]{0,1:T(8,128)(2,1)}, u32[]{:S(2)}) copy-start(bf16[1024,2048]{0,1:T(8,128)(2,1)} %all-gather.2.cloned.1.call-done) | copy-start | bytes 12582916
  81.1 4.1 %copy-start.2 = (bf16[1024,2048]{0,1:T(8,128)(2,1)S(1)}, bf16[1024,2048]{0,1:T(8,128)(2,1)}, u32[]{:S(2)}) copy-start(bf16[1024,2048]{0,1:T(8,128)(2,1)} %all-gather.2.cloned.1.call-done) | copy-start | bytes 12582916
  81.1 4.1 %copy-start.4 = (bf16[2048,256]{1,0:T(8,128)(2,1)S(1)}, bf16[2048,256]{1,0:T(8,128)(2,1)}, u32[]{:S(2)}) copy-start(bf16[2048,256]{1,0:T(8,128)(2,1)} %param.22) | copy-start | bytes 3145732
  81.2 5.9 %slice-start = ((s8[8388608]{0:T(1024)(128)(4,1)}), s8[4194304]{0:T(1024)(128)(4,1)S(1)}, s32[]{:S(2)}) async-start(s8[8388608]{0:T(1024)(128)(4,1)} %bitcast.77), calls=%async_computation.2 | async-start | bytes 8388608
  85.3 2.4 %slice-start.1 = ((s8[8388608]{0:T(1024)(128)(4,1)}), s8[4194304]{0:T(1024)(128)(4,1)S(1)}, s32[]{:S(2)}) async-start(s8[8388608]{0:T(1024)(128)(4,1)} %bitcast.77), calls=%async_computation.3 | async-start | bytes 8388608
  105.6 4.4 %collective-permute-start = (bf16[1024,1024]{1,0:T(8,128)(2,1)S(1)}, bf16[1024,1024]{1,0:T(8,128)(2,1)}, u32[]{:S(2)}, u32[]{:S(2)}) collective-permute-start(bf16[1024,1024]{1,0:T(8,128)(2,1)S(1)} %convolution_convert_fusion), channel_id=1, source_target_pairs={{0,1},{1,0},{2,3},{3,2},{4,5},{5,4},{6,7},{7,6},{8,9},{9,8},{10,11... | collective-permute-start | bytes 6291464 | tf_op jit(solution)/shard_map/ppermute | solution.py:244
  112.4 32.9 %copy-start.9 = (bf16[64]{0:T(256)(128)(2,1)S(1)}, bf16[64]{0:T(256)(128)(2,1)}, u32[]{:S(2)}) copy-start(bf16[64]{0:T(256)(128)(2,1)} %param.32) | copy-start | bytes 388
  113.5 25.5 %collective-permute-start.1 = (bf16[8,64,1024]{2,1,0:T(8,128)(2,1)}, bf16[8,64,1024]{2,1,0:T(8,128)(2,1)}, u32[]{:S(2)}, u32[]{:S(2)}) collective-permute-start(bf16[8,64,1024]{2,1,0:T(8,128)(2,1)} %dynamic-slice_bitcast_fusion), channel_id=1, source_target_pairs={{0,2},{1,3},{2,0},{3,1},{4,6},{5,7},{6,4},{7,5},{8,10},{9,11},{10,... | collective-permute-start | bytes 3145736 | tf_op jit(solution)/shard_map/ppermute | solution.py:251
  141.7 29.1 %all-to-all-start = ((bf16[8,64,1024]{2,1,0:T(8,128)(2,1)}), bf16[8,64,1024]{2,1,0:T(8,128)(2,1)S(1)}, u32[]{:S(2)}, u32[]{:S(2)}) async-start(bf16[8,64,1024]{2,1,0:T(8,128)(2,1)} %fusion.3), calls=%async_computation | async-start | bytes 2097152 | tf_op jit(solution)/shard_map/all_to_all | solution.py:257
Sparse Core Ops, SparseCore 0:
  11.4 64.4 all-gather.1
where the time goes:
time: 218 us; the launch traced here: 216 us
  waiting for transfers between devices  108 us (50%)
  blocking collectives  44.4 us (20%)
  between operations  14.5 us (7%)
  local copies, waits for them, and re-layouts  13.8 us (6%)
  matrix products  11.3 us (5%)
  other arithmetic  10.6 us (5%)
  Pallas kernels  9.3 us (4%)
  starting transfers between devices  4.49 us (2%)
    all_gather x1, waiting for transfers between devices, on_device(): gathered = lax.all_gather(order(tokens), AXES, axis=1, tiled=True)  54.5 us
    psum x1, blocking collectives, on_device(): sumsq = lax.psum(jnp.sum(share * share, axis=0), AXES)  37.5 us
    all_to_all x1, waiting for transfers between devices, scattered_sum(): parts = lax.all_to_all(summed, 'kv', 0, 0, tiled=True)  25.5 us
    ppermute x1, waiting for transfers between devices, scattered_sum(): other = lax.ppermute(other, 'tp', across)  24.7 us
    pallas_call x1, Pallas kernels, delta_call(): pl.pallas_call(functools.partial(delta_kernel, prop), grid=(tiles, heads)...  9.3 us
    psum x1, blocking collectives, on_device(): squares = lax.psum(squares.reshape(heads, rows), 'tp')  6.85 us
  transfers between devices with their start and end apart: 4, of which 4 were waited for; matrix products, arithmetic and copies ran while one was open for 6% of the time, Pallas kernels for 0%

commit v1 on v0

v1 whole, which is shorter than its diff:
```python
import functools

import jax
import jax.numpy as jnp
from jax import lax
from jax.experimental import pallas as pl
from jax.experimental.pallas import tpu as pltpu
from jax.sharding import PartitionSpec as P

epsilon = 1e-06
GROUP = 16
AXES = ("kv", "tp")
MESH = pl.DeviceIdType.MESH
f32, bf16 = jnp.float32, jnp.bfloat16


class Grid:
    def __init__(self, kv, tp):
        self.kv, self.tp = kv, tp
        self.x = tp // 2
        self.y = self.x if kv % self.x == 0 else 1
        self.z = kv // self.y
        self.sizes = (self.z, self.y, self.x)

    def here(self):
        kv, tp = lax.axis_index("kv"), lax.axis_index("tp")
        self.at = (kv // self.y, lax.rem(kv, self.y), tp // 2)
        self.core = lax.rem(tp, 2)

    def shift(self, offset):
        return tuple(lax.rem(a + o % n, n) for a, o, n in zip(self.at, offset, self.sizes))

    def device(self, offset, flip=0):
        z, y, x = self.shift(offset)
        core = 1 - self.core if flip else self.core
        return (z * self.y + y, x * 2 + core)

    def chip(self, offset):
        z, y, x = self.shift(offset)
        return (z * self.y + y) * self.x + x

    def group(self, offset):
        z, y, _ = self.shift(offset)
        return z * self.y + y


def offsets(sizes):
    return [(a, b, c) for a in range(sizes[0]) for b in range(sizes[1]) for c in range(sizes[2])]


def negated(offset, sizes):
    return tuple(-o % n for o, n in zip(offset, sizes))


def meet(grid, peers):
    peers = set(peers) | {(negated(o, grid.sizes), f) for o, f in peers}
    peers = sorted(peers - {((0, 0, 0), 0)})
    barrier = pltpu.get_barrier_semaphore()
    for offset, flip in peers:
        pl.semaphore_signal(
            barrier, inc=1, device_id=grid.device(offset, flip), device_id_type=MESH
        )
    pl.semaphore_wait(barrier, len(peers))


def remote(src, dst, send, recv, device):
    return pltpu.make_async_remote_copy(
        src_ref=src, dst_ref=dst, send_sem=send, recv_sem=recv, device_id=device,
        device_id_type=MESH,
    )


def tree(sizes, order):
    first, second, third = order
    steps = []
    for offset in offsets(sizes):
        onward = []
        if offset[second] == 0 and offset[third] == 0 and offset[first] < sizes[first] - 1:
            onward.append(first)
        if offset[third] == 0 and offset[second] < sizes[second] - 1:
            onward.append(second)
        if offset[third] < sizes[third] - 1:
            onward.append(third)
        steps.append((offset, onward))
    return steps


def unit(dim, sign):
    return tuple(sign if d == dim else 0 for d in range(3))


def plan(sizes, orders, pieces, stagger):
    events = []
    for p in range(pieces):
        for half, (order, sign) in enumerate(orders):
            for offset, onward in tree(sizes, order):
                events.append((sum(offset) + stagger * p, p, half, offset, onward))
    return sorted(events, key=lambda e: (e[0], e[1], e[3], e[2]))


class Spread:
    def __init__(self, grid, sizes, orders, pieces, stagger, place, halves, send, recv, both):
        self.grid, self.sizes, self.orders, self.pieces = grid, sizes, orders, pieces
        self.place, self.halves = place, halves
        self.send, self.recv, self.both = send, recv, both
        self.events = plan(sizes, orders, pieces, stagger)

    def slot(self, offset):
        a, b, c = offset
        return (a * self.sizes[1] + b) * self.sizes[2] + c

    def source(self, half, offset):
        sign = self.orders[half][1]
        return tuple(-sign * o for o in offset)

    def view(self, p, half, offset):
        return self.place(p, half, self.source(half, offset), self.grid.core)

    def copy(self, p, half, offset, dim):
        sign = self.orders[half][1]
        landed = tuple(o + (1 if d == dim else 0) for d, o in enumerate(offset))
        here = self.view(p, half, offset)
        return remote(
            here, here, self.send.at[p], self.recv.at[p, half, self.slot(landed)],
            self.grid.device(unit(dim, sign)),
        )

    def share(self, p, half, offset):
        here = self.view(p, half, offset)
        return remote(
            here, here, self.both.at[0, p], self.both.at[1, p], self.grid.device((0, 0, 0), 1)
        )

    def run(self, finish):
        left = [0] * self.pieces
        for _, p, half, offset, onward in self.events:
            left[p] += 1
        for _, p, half, offset, onward in self.events:
            if any(offset):
                here = self.view(p, half, offset)
                remote(
                    here, here, self.send.at[p], self.recv.at[p, half, self.slot(offset)],
                    self.grid.device((0, 0, 0), 1),
                ).wait_recv()
                for dim in onward:
                    self.copy(p, half, offset, dim).start()
                self.share(p, half, offset).start()
            left[p] -= 1
            if left[p] == 0:
                finish(p)

    def begin(self, p):
        for _, q, half, offset, onward in self.events:
            if q == p and not any(offset):
                for dim in onward:
                    self.copy(p, half, offset, dim).start()
                self.share(p, half, offset).start()

    def shared(self, p, whole):
        remote(whole, whole, self.both.at[0, p], self.both.at[1, p],
               self.grid.device((0, 0, 0), 1)).wait_recv()

    def sent(self, p, whole, rest):
        far = self.grid.device((0, 0, 0), 1)
        remote(rest, rest, self.send.at[p], self.both.at[1, p], far).wait_send()
        remote(whole, whole, self.both.at[0, p], self.both.at[1, p], far).wait_send()


ORDERS = (((0, 1, 2), 1), ((0, 2, 1), -1))
FLAT = (((0, 1, 2), 1), ((0, 1, 2), -1))
STAGGER = 2


def project_kernel(
    kv, tp,
    tok, gain, wq, wk, wv, wz, ws, wd, rate, extra, old_strength, old_decay, accepted, parent, wo,
    q_out, k_out, v_out, z_out, sc_out, wx_out,
    xt, wt, gcol, wqk, wout, wx, local, send, recv, both, wsend, wrecv,
):
    grid = Grid(kv, tp)
    grid.here()
    pieces, own, seqs = tok.shape
    width = gain.shape[1]
    cols = wq.shape[1]
    small = wv.shape[0]
    heads = rate.shape[1]
    hd = cols // heads
    part = wout.shape[1] // kv
    half_width = seqs // 2

    def place(p, half, offset, core):
        return xt.at[p, grid.chip(offset), core, :, pl.ds(half * half_width, half_width)]

    loads = [
        pltpu.make_async_copy(tok, xt.at[:, grid.chip((0, 0, 0)), grid.core], local.at[0]),
        pltpu.make_async_copy(wo, wout, local.at[1]),
        pltpu.make_async_copy(wq, wqk.at[0], local.at[2]),
        pltpu.make_async_copy(wk, wqk.at[1], local.at[3]),
        pltpu.make_async_copy(wv, wt.at[pl.ds(2 * cols, small)], local.at[4]),
        pltpu.make_async_copy(wz, wt.at[pl.ds(2 * cols + small, small)], local.at[5]),
    ]
    for load in loads:
        load.start()

    plane = [o for o in offsets((grid.z, grid.y, 1)) if any(o)]
    peers = [(unit(d, s), 0) for d in range(3) for s in (1, -1) if grid.sizes[d] > 1]
    peers = [(tuple(o % n for o, n in zip(off, grid.sizes)), f) for off, f in peers]
    peers += [(o, 0) for o in plane] + [((0, 0, 0), 1)]
    meet(grid, peers)

    spread = Spread(
        grid, grid.sizes, ORDERS, pieces, STAGGER, place, 2, send, recv, both
    )
    loads[0].wait()
    for p in range(pieces):
        spread.begin(p)
    loads[1].wait()
    mine = grid.group((0, 0, 0))
    for index, offset in enumerate(plane):
        start = pl.multiple_of(grid.group(offset) * part, part)
        remote(
            wout.at[:, pl.ds(start, part)], wx.at[mine, grid.core],
            wsend.at[0], wrecv.at[index], grid.device(offset),
        ).start()
    wx[mine, grid.core] = wout[:, pl.ds(pl.multiple_of(mine * part, part), part)]

    for first in range(0, width, 128):
        piece = gain[:, first : first + 128].astype(f32)
        gcol[first : first + 128, :] = jnp.broadcast_to(piece, (128, 128)).T
    loads[2].wait()
    loads[3].wait()
    for which in range(2):
        for first in range(0, width, 256):
            piece = wqk[which, first : first + 256, :].astype(f32)
            wt[which * cols : (which + 1) * cols, first : first + 256] = piece.T.astype(bf16)
    loads[4].wait()
    loads[5].wait()
    tail = wt.shape[0] - 2 * cols - 2 * small
    rows = [ws[...].astype(f32), wd[...].astype(f32)]
    rows.append(jnp.zeros((tail - 2 * heads, width), f32))
    wt[2 * cols + 2 * small :, :] = jnp.concatenate(rows, axis=0).astype(bf16)

    chips = kv * tp // 2

    def finish(p):
        spread.shared(p, xt.at[p, :, 1 - grid.core])
        x = xt[p].reshape(width, seqs).astype(f32)
        square = jnp.sum(x * x, axis=0, keepdims=True)
        scale = lax.rsqrt(square / width + epsilon)
        g = jnp.concatenate([gcol[...]] * (seqs // 128), axis=1)
        normed = (x * scale * g).astype(bf16)
        out = jnp.dot(wt[...], normed, preferred_element_type=f32)
        for index, ref in enumerate((q_out, k_out)):
            ref[p] = out[index * cols : (index + 1) * cols].T.astype(bf16)
        v_out[p] = out[2 * cols : 2 * cols + small].astype(bf16)
        z_out[p] = out[2 * cols + small : 2 * cols + 2 * small].astype(bf16)
        side = out[2 * cols + 2 * small :]
        live = jnp.where(accepted[...] > p, 1.0, 0.0)
        for h in range(heads):
            strength = side[h : h + 1]
            decay = side[heads + h : heads + h + 1]
            beta = 1.0 / (1.0 + jnp.exp(-strength))
            soft = jnp.maximum(decay, 0.0) + jnp.log1p(jnp.exp(-jnp.abs(decay)))
            g_new = -rate[0:1, h : h + 1] * soft + extra[p, h : h + 1, :]
            zero = jnp.zeros((1, seqs), f32)
            sc_out[p, h] = jnp.concatenate(
                [
                    old_strength[p, h : h + 1, :] * live,
                    old_decay[p, h : h + 1, :] * live,
                    beta,
                    g_new,
                    parent[p : p + 1, :].astype(f32),
                    zero, zero, zero,
                ],
                axis=0,
            )

    spread.run(finish)

    for index, offset in enumerate(plane):
        origin = grid.group(negated(offset, grid.sizes))
        here = wx.at[origin, grid.core]
        remote(here, here, wsend.at[0], wrecv.at[index], grid.device(offset)).wait_recv()
        remote(here, here, wsend.at[1], wrecv.at[len(plane)],
               grid.device((0, 0, 0), 1)).start()
    here = wout.at[:, pl.ds(pl.multiple_of(mine * part, part), part)]
    remote(here, wx.at[mine, grid.core], wsend.at[1], wrecv.at[len(plane)],
           grid.device((0, 0, 0), 1)).start()
    far = grid.device((0, 0, 0), 1)
    other = wx.at[:, 1 - grid.core]
    remote(other, other, wsend.at[1], wrecv.at[len(plane)], far).wait()
    rest = wx.at[pl.ds(0, kv - 1), 0]
    remote(rest, rest, wsend.at[0], wrecv.at[0], far).wait_send()
    for p in range(pieces):
        spread.sent(p, xt.at[p, :, 0], xt.at[p, pl.ds(0, chips - 1), 0])
    wx_out[...] = wx[...]


def project(kv, tp, width, tokens, gain, wq, wk, wv, wz, ws, wd, rate, extra, strength, decay,
            accepted, parent, wo):
    pieces, own, seqs = tokens.shape
    cols = wq.shape[1]
    small = wv.shape[0]
    heads = rate.shape[1]
    chips = kv * tp // 2
    part = wo.shape[1] // kv
    rows = 2 * cols + 2 * small + 16 * -(-2 * heads // 16)
    vmem, anyw = pltpu.VMEM, pl.ANY
    spec = lambda space: pl.BlockSpec(memory_space=space)
    grid = Grid(kv, tp)
    return pl.pallas_call(
        functools.partial(project_kernel, kv, tp),
        in_specs=[spec(s) for s in (
            anyw, vmem, anyw, anyw, anyw, anyw, vmem, vmem, vmem, vmem, vmem, vmem, vmem, vmem, anyw
        )],
        out_specs=[spec(vmem)] * 6,
        out_shape=[
            jax.ShapeDtypeStruct((pieces, seqs, cols), bf16),
            jax.ShapeDtypeStruct((pieces, seqs, cols), bf16),
            jax.ShapeDtypeStruct((pieces, small, seqs), bf16),
            jax.ShapeDtypeStruct((pieces, small, seqs), bf16),
            jax.ShapeDtypeStruct((pieces, heads, 8, seqs), f32),
            jax.ShapeDtypeStruct((kv, 2, wo.shape[0], part), bf16),
        ],
        scratch_shapes=[
            pltpu.VMEM((pieces, chips, 2, own, seqs), bf16),
            pltpu.VMEM((rows, width), bf16),
            pltpu.VMEM((width, 128), f32),
            pltpu.VMEM((2, width, cols), bf16),
            pltpu.VMEM(wo.shape, bf16),
            pltpu.VMEM((kv, 2, wo.shape[0], part), bf16),
            pltpu.SemaphoreType.DMA((6,)),
            pltpu.SemaphoreType.DMA((pieces,)),
            pltpu.SemaphoreType.DMA((pieces, 2, chips)),
            pltpu.SemaphoreType.DMA((2, pieces)),
            pltpu.SemaphoreType.DMA((2,)),
            pltpu.SemaphoreType.DMA((kv,)),
        ],
        compiler_params=pltpu.CompilerParams(
            collective_id=0, has_side_effects=True, vmem_limit_bytes=48 * 1024 * 1024
        ),
        cost_estimate=pl.CostEstimate(
            flops=2 * rows * width * pieces * seqs, bytes_accessed=8 << 20, transcendentals=0
        ),
    )(tokens, gain, wq, wk, wv, wz, ws, wd, rate, extra, strength, decay, accepted, parent, wo)


def total(terms):
    terms = list(terms)
    while len(terms) > 1:
        terms = [sum(terms[i : i + 2][1:], terms[i]) for i in range(0, len(terms), 2)]
    return terms[0]


def delta_kernel(
    prop, q_ref, k_ref, ok_ref, v_ref, ov_ref, z_ref, sc_ref, hg_ref, s_ref,
    o_ref, sq_ref, out_ref, kt_ref, eg_ref,
):
    lanes = s_ref.shape[0]
    vdim = s_ref.shape[2]
    hd = s_ref.shape[3]
    groups = lanes // GROUP

    for index, ref in enumerate((ok_ref, k_ref, q_ref)):
        for p in range(prop):
            tile = ref[p].astype(f32)
            kt_ref[index * prop + p] = tile.T
    positions = 2 * prop
    square = [jnp.sum(kt_ref[i] * kt_ref[i], axis=0, keepdims=True) for i in range(3 * prop)]
    inv = [lax.rsqrt(x + epsilon) for x in square]
    inv = inv[:positions] + [x * hd ** (-0.5) for x in inv[positions:]]

    def scalar(row, p):
        return sc_ref[p, 0, row : row + 1, :]

    beta = [scalar(0, p) for p in range(prop)] + [scalar(2, p) for p in range(prop)]
    g = [scalar(1, p) for p in range(prop)] + [scalar(3, p) for p in range(prop)]
    parents = [scalar(4, p) for p in range(prop)]
    ancestor = []
    for i in range(prop):
        direct = [jnp.where(parents[i] == float(j), 1.0, 0.0) for j in range(i)]
        row = []
        for j in range(i):
            row.append(total([direct[j]] + [direct[m] * ancestor[m][j] for m in range(j + 1, i)]))
        ancestor.append(row)

    def vis(i, j):
        if i < prop or j < prop:
            return None
        return ancestor[i - prop][j - prop]

    gam = []
    for i in range(positions):
        acc = g[i]
        for j in range(i):
            seen = vis(i, j)
            acc = acc + (g[j] if seen is None else seen * g[j])
        gam.append(acc)
    eg = [jnp.exp(x) for x in gam]

    def decay(i, j):
        value = jnp.exp(jnp.minimum(gam[i] - gam[j], 0.0))
        seen = vis(i, j)
        return value if seen is None else value * seen

    def gram(i, j):
        return jnp.sum(kt_ref[i] * kt_ref[j], axis=0, keepdims=True) * (inv[i] * inv[j])

    dec = {(i, j): decay(i, j) for i in range(positions) for j in range(i)}
    coupling = {(i, j): beta[i] * gram(i, j) * dec[i, j] for (i, j) in dec}
    reach = {}
    for p in range(prop):
        i = prop + p
        for j in range(i + 1):
            value = gram(positions + p, j)
            reach[p, j] = value if j == i else value * dec[i, j]

    last = eg[prop - 1]
    eg_ref[...] = jnp.broadcast_to(last, (lanes, lanes)).T

    lane = lax.broadcasted_iota(jnp.int32, (vdim, lanes), 1)
    inner, outer = lane % GROUP, lane // GROUP
    products = []
    for c in range(groups):
        rows = s_ref[c * GROUP : (c + 1) * GROUP, 0].reshape(GROUP * vdim, hd).astype(bf16)
        tiles = []
        for ref in (ok_ref, k_ref, q_ref):
            for p in range(prop):
                start = c * GROUP
                tiles.append(ref[p, start : start + GROUP, :])
        keys = jnp.concatenate(tiles, axis=0)
        product = lax.dot_general(
            rows, keys, (((1,), (1,)), ((), ())), preferred_element_type=f32
        )
        wide = []
        for first in range(0, 3 * prop * GROUP, lanes):
            width = min(lanes, 3 * prop * GROUP - first)
            part = product[:, first : first + width]
            chosen = part[:vdim]
            for s in range(1, GROUP):
                mask = (inner if width == lanes else inner[:, :width]) == s
                chosen = jnp.where(mask, part[s * vdim : (s + 1) * vdim], chosen)
            if width < lanes:
                chosen = jnp.concatenate(
                    [chosen, jnp.zeros((vdim, lanes - width), f32)], axis=1
                )
            wide.append(chosen)
        products.append(wide)

    per_tile = lanes // GROUP

    def swap(source, sources, targets):
        shifted = []
        for d in range(groups):
            acc = None
            for a in range(sources):
                t = (a - d) % groups
                if t >= targets:
                    continue
                acc = source[a] if acc is None else jnp.where(outer == t, source[a], acc)
            shifted.append(acc if acc is None or d == 0 else pltpu.roll(acc, d * GROUP, 1))
        results = []
        for t in range(targets):
            acc = None
            for a in range(sources):
                piece = shifted[(a - t) % groups]
                acc = piece if acc is None else jnp.where(outer == a, piece, acc)
            results.append(acc)
        return results

    raw = []
    for tile in range(len(products[0])):
        count = min(per_tile, 3 * prop - tile * per_tile)
        raw += swap([products[c][tile] for c in range(groups)], groups, count)

    update = []
    for i in range(positions):
        source = ov_ref if i < prop else v_ref
        value = source[i % prop].astype(f32)
        acc = beta[i] * value - (beta[i] * eg[i] * inv[i]) * raw[i]
        for j in range(i):
            acc = acc - coupling[i, j] * update[j]
        update.append(acc)

    for p in range(prop):
        i = prop + p
        acc = (eg[i] * inv[positions + p]) * raw[positions + p]
        for j in range(i + 1):
            acc = acc + reach[p, j] * update[j]
        sq_ref[0, p : p + 1, :] = jnp.sum(acc * acc, axis=0, keepdims=True)
        gate = z_ref[p].astype(f32)
        gate = gate / (1.0 + jnp.exp(-gate))
        o_ref[p] = acc * hg_ref[...] * gate

    weighted = [
        update[j] * (jnp.exp(gam[prop - 1] - gam[j]) * inv[j]) for j in range(prop)
    ]
    compact = swap(weighted, prop, groups)
    width = prop * GROUP
    narrow = inner[:, :width]
    for c in range(groups):
        tiles = [ok_ref[p, c * GROUP : (c + 1) * GROUP, :] for p in range(prop)]
        keys = jnp.concatenate(tiles, axis=0)
        piece = compact[c][:, :width]
        left = jnp.concatenate(
            [jnp.where(narrow == s, piece, 0.0) for s in range(GROUP)], axis=0
        ).astype(bf16)
        delta = jnp.dot(left, keys, preferred_element_type=f32)
        for s in range(GROUP):
            seq = c * GROUP + s
            out_ref[seq, 0] = (
                s_ref[seq, 0] * eg_ref[seq : seq + 1, :hd] + delta[s * vdim : (s + 1) * vdim]
            )


def delta_call(lanes, q, k, ok, v, ov, z, scal, hgain, state):
    seqs, heads, vdim, hd = state.shape
    prop = q.shape[0]
    tiles = seqs // lanes
    natural = pl.BlockSpec((prop, lanes, hd), lambda t, h: (0, t, h))
    turned = pl.BlockSpec((prop, vdim, lanes), lambda t, h: (0, h, t))
    state_spec = pl.BlockSpec((lanes, 1, vdim, hd), lambda t, h: (t, h, 0, 0))
    return pl.pallas_call(
        functools.partial(delta_kernel, prop),
        grid=(tiles, heads),
        in_specs=[
            natural,
            natural,
            natural,
            turned,
            turned,
            turned,
            pl.BlockSpec((prop, 1, 8, lanes), lambda t, h: (0, h, 0, t)),
            pl.BlockSpec((vdim, lanes), lambda t, h: (0, 0)),
            state_spec,
        ],
        out_specs=[
            turned,
            pl.BlockSpec((1, prop, lanes), lambda t, h: (h, 0, t)),
            state_spec,
        ],
        out_shape=[
            jax.ShapeDtypeStruct((prop, heads * vdim, seqs), f32),
            jax.ShapeDtypeStruct((heads, prop, seqs), f32),
            jax.ShapeDtypeStruct(state.shape, f32),
        ],
        scratch_shapes=[
            pltpu.VMEM((3 * prop, hd, lanes), f32),
            pltpu.VMEM((lanes, lanes), f32),
        ],
        compiler_params=pltpu.CompilerParams(vmem_limit_bytes=40 * 1024 * 1024),
        cost_estimate=pl.CostEstimate(
            flops=2 * seqs * heads * vdim * hd * 256,
            bytes_accessed=8 * seqs * heads * vdim * hd,
            transcendentals=0,
        ),
    )(q, k, ok, v, ov, z, scal, hgain, state)


def output_kernel(
    kv, tp, hd,
    m_ref, sq_ref, wx_ref, gain_ref,
    out_ref,
    squares, xb, wt, mine, parts, sums, local, qsend, qrecv, send, recv, both, psend, precv,
    ssend, srecv,
):
    grid = Grid(kv, tp)
    grid.here()
    pieces, chans, seqs = m_ref.shape
    heads = sq_ref.shape[0]
    vdim = chans // heads
    own = out_ref.shape[1]
    feats = wx_ref.shape[3]
    half_width = seqs // 2
    everyone = [(o, f) for o in offsets(grid.sizes) for f in (0, 1)]
    everyone = [e for e in everyone if any(e[0]) or e[1]]
    meet(grid, everyone)

    row = [(o, f) for o, f in everyone if not o[0] and not o[1]]
    column = lax.axis_index("tp")
    for index, (offset, flip) in enumerate(row):
        remote(
            sq_ref, squares.at[column], qsend.at[index], qrecv.at[index],
            grid.device(offset, flip),
        ).start()
    squares[column] = sq_ref[...]
    for first in range(0, kv):
        piece = wx_ref[first].reshape(2 * chans, feats).astype(f32)
        wt[first] = piece.T.astype(bf16)

    def place(p, half, offset, core):
        return xb.at[p, grid.group(offset), core, :, pl.ds(half * half_width, half_width)]

    for index, (offset, flip) in enumerate(row):
        remote(
            sq_ref, squares.at[column], qsend.at[index], qrecv.at[index],
            grid.device(offset, flip),
        ).wait()
    sizes = (grid.z, grid.y, 1)
    spread = Spread(grid, sizes, FLAT, pieces, STAGGER, place, 2, send, recv, both)
    everything = squares[0]
    for index in range(1, tp):
        everything = everything + squares[index]
    scale = lax.rsqrt(everything / hd + epsilon)
    mine_kv = grid.group((0, 0, 0))
    for p in range(pieces):
        turned = [
            m_ref[p, h * vdim : (h + 1) * vdim, :] * scale[h, p : p + 1, :] for h in range(heads)
        ]
        xb[p, mine_kv, grid.core] = jnp.concatenate(turned, axis=0).astype(bf16)
        spread.begin(p)

    line = [(0, 0, c) for c in range(1, grid.x)]
    depth = kv * 2 * chans

    def finish(p):
        spread.shared(p, xb.at[p, :, 1 - grid.core])
        out = None
        for g in range(kv):
            term = jnp.dot(
                wt[g], xb[p, g].reshape(2 * chans, seqs), preferred_element_type=f32
            )
            out = term if out is None else out + term
        parts[p] = out.reshape(feats // own, own, seqs)
        for index, offset in enumerate(line):
            far = grid.shift(offset)[2] * 2 + grid.core
            remote(
                parts.at[p, far], mine.at[p, index], psend.at[p, index], precv.at[p, index],
                grid.device(offset),
            ).start()

    spread.run(finish)
    slot = grid.at[2] * 2 + grid.core
    me = lax.axis_index("kv") * tp + column
    for p in range(pieces):
        acc = parts[p, slot]
        for index, offset in enumerate(line):
            far = grid.shift(offset)[2] * 2 + grid.core
            remote(
                parts.at[p, far], mine.at[p, index], psend.at[p, index], precv.at[p, index],
                grid.device(offset),
            ).wait()
            acc = acc + mine[p, index]
        parts[p, slot] = acc
        sums[me, p : p + 1, :] = jnp.sum(acc * acc, axis=0, keepdims=True)
    for index, (offset, flip) in enumerate(everyone):
        remote(
            sums.at[me], sums.at[me], ssend.at[0], srecv.at[index], grid.device(offset, flip)
        ).start()
    for index, (offset, flip) in enumerate(everyone):
        z, y, x = grid.shift(negated(offset, grid.sizes))
        core = 1 - grid.core if flip else grid.core
        origin = (z * grid.y + y) * tp + x * 2 + core
        remote(
            sums.at[origin], sums.at[origin], ssend.at[0], srecv.at[index],
            grid.device(offset, flip),
        ).wait_recv()
    summed = jnp.sum(sums[...], axis=0)
    final = lax.rsqrt(summed / (kv * tp * own) + epsilon)
    g = gain_ref[...]
    for p in range(pieces):
        out_ref[p] = (parts[p, slot] * final[p : p + 1, :] * g).astype(bf16)
    rest = sums.at[pl.ds(0, kv * tp - 1)]
    far = grid.device((0, 0, 0), 1)
    remote(rest, rest, ssend.at[0], srecv.at[0], far).wait_send()
    for p in range(pieces):
        spread.sent(p, xb.at[p, :, 0], xb.at[p, pl.ds(0, kv - 1), 0])


def output(kv, tp, hd, own, m, sq, wx, gain):
    pieces, chans, seqs = m.shape
    heads = sq.shape[0]
    feats = wx.shape[3]
    x = tp // 2
    spec = pl.BlockSpec(memory_space=pltpu.VMEM)
    peers = kv * tp - 1
    return pl.pallas_call(
        functools.partial(output_kernel, kv, tp, hd),
        in_specs=[spec] * 4,
        out_specs=spec,
        out_shape=jax.ShapeDtypeStruct((pieces, own, seqs), bf16),
        scratch_shapes=[
            pltpu.VMEM((tp, heads, pieces, seqs), f32),
            pltpu.VMEM((pieces, kv, 2, chans, seqs), bf16),
            pltpu.VMEM((kv, feats, 2 * chans), bf16),
            pltpu.VMEM((pieces, max(x - 1, 1), own, seqs), f32),
            pltpu.VMEM((pieces, feats // own, own, seqs), f32),
            pltpu.VMEM((kv * tp, pieces, seqs), f32),
            pltpu.SemaphoreType.DMA((1,)),
            pltpu.SemaphoreType.DMA((tp,)),
            pltpu.SemaphoreType.DMA((tp,)),
            pltpu.SemaphoreType.DMA((pieces,)),
            pltpu.SemaphoreType.DMA((pieces, 2, kv)),
            pltpu.SemaphoreType.DMA((2, pieces)),
            pltpu.SemaphoreType.DMA((pieces, max(x - 1, 1))),
            pltpu.SemaphoreType.DMA((pieces, max(x - 1, 1))),
            pltpu.SemaphoreType.DMA((1,)),
            pltpu.SemaphoreType.DMA((peers,)),
        ],
        compiler_params=pltpu.CompilerParams(
            collective_id=1, has_side_effects=True, vmem_limit_bytes=32 * 1024 * 1024
        ),
        cost_estimate=pl.CostEstimate(
            flops=2 * feats * kv * 2 * chans * pieces * seqs, bytes_accessed=4 << 20,
            transcendentals=0,
        ),
    )(m, sq, wx, gain)


def on_device(
    kv,
    tp,
    tokens,
    input_norm_gain,
    query_weight,
    key_weight,
    value_weight,
    output_gate_weight,
    strength_weight,
    decay_weight,
    head_decay_rate,
    proposal_log_decay,
    head_norm_gain,
    output_weight,
    output_norm_gain,
    state,
    previous_keys,
    previous_values,
    previous_log_decay,
    previous_strengths,
    accepted,
    parent,
):
    seqs, heads, vdim, hd = state.shape
    prop = parent.shape[1]
    width = input_norm_gain.shape[0]
    lanes = min(128, seqs)
    own = tokens.shape[2]
    channels = heads * vdim

    def turn(x):
        return jnp.transpose(x, (1, 2, 0))

    q, k, v, z, scal, wx = project(
        kv, tp, width,
        turn(tokens),
        input_norm_gain[None, :],
        query_weight,
        key_weight,
        turn(value_weight).reshape(channels, width),
        turn(output_gate_weight).reshape(channels, width),
        strength_weight.T,
        decay_weight.T,
        head_decay_rate[None, :],
        turn(proposal_log_decay),
        turn(previous_strengths),
        turn(previous_log_decay),
        accepted[None, :],
        parent.T,
        output_weight.reshape(channels, width),
    )
    old_keys = jnp.transpose(previous_keys, (1, 0, 2))
    old_values = jnp.transpose(previous_values, (1, 2, 3, 0)).reshape(prop, channels, seqs)
    hgain = jnp.broadcast_to(head_norm_gain.astype(f32)[:, None], (vdim, lanes))
    m, sq, accepted_state = delta_call(
        lanes, q, k, old_keys, v, old_values, z, scal, hgain, state
    )
    ogain = jnp.broadcast_to(output_norm_gain.astype(f32)[:, None], (own, seqs))
    layer_out = output(kv, tp, hd, own, m, sq, wx, ogain)
    return (jnp.transpose(layer_out, (2, 0, 1)), accepted_state)


def solution(mesh):
    placed = (
        P(None, None, AXES),
        P(),
        P(None, "kv"),
        P(None, "kv"),
        P(None, "kv", "tp"),
        P(None, "kv", "tp"),
        P(None, "kv"),
        P(None, "kv"),
        P("kv"),
        P(None, None, "kv"),
        P("tp"),
        P("kv", "tp", None),
        P(AXES),
        P(None, "kv", "tp", None),
        P(None, None, "kv"),
        P(None, None, "kv", "tp"),
        P(None, None, "kv"),
        P(None, None, "kv"),
        P(),
        P(),
    )
    return jax.shard_map(
        functools.partial(on_device, mesh.shape["kv"], mesh.shape["tp"]),
        mesh=mesh,
        in_specs=placed,
        out_specs=(P(None, None, AXES), P(None, "kv", "tp", None)),
        check_vma=False,
    )
```

time: 218 us -> 132 us (0.61)
  waiting for transfers between devices: 108 us -> 0 us
  Pallas kernels: 9.3 us -> 117 us
  blocking collectives: 44.4 us -> 0 us
  between operations: 14.5 us -> 0.71 us
  matrix products: 11.3 us -> 0 us
  other arithmetic: 10.6 us -> 0 us
  starting transfers between devices: 4.49 us -> 0 us
    pallas_call x0 -> x2, Pallas kernels: none -> 107 us  [the longest x1 54.9 us: project(): pl.pallas_call(functools.partial(project_kernel, kv, tp), in_specs=[spec(...]
    all_gather x1 -> x0, waiting for transfers between devices: 54.5 us -> none  [on_device(): gathered = lax.all_gather(order(tokens), AXES, axis=1, tiled=True)]
    psum x2 -> x0, blocking collectives: 44.4 us -> none  [the longest x1 37.5 us: on_device(): sumsq = lax.psum(jnp.sum(share * share, axis=0), AXES)]
    ppermute x2 -> x0, waiting for transfers between devices: 28.1 us -> none  [the longest x1 24.7 us: scattered_sum(): other = lax.ppermute(other, 'tp', across)]
    all_to_all x1 -> x0, waiting for transfers between devices: 25.5 us -> none  [scattered_sum(): parts = lax.all_to_all(summed, 'kv', 0, 0, tiled=True)]
    unnamed x25 -> x40, local copies, waits for them, and re-layouts: 0.79 us -> 13.1 us
    dot_general x5 -> x0, matrix products: 11.3 us -> none  [the longest x1 4.09 us: on_device(): keys = jnp.dot(normed, key_weight, preferred_element_type=f32).astype(bf16)]
    reshape x19 -> x0, local copies, waits for them, and re-layouts: 6.51 us -> none  [the longest x11 3.19 us: order(): x = x.reshape((tiles, lanes, prop) + tail)]
  transfers between devices with their start and end apart: 4 -> 0, of which waited for: 4 -> 0; matrix products, arithmetic and copies ran while one was open for 6% -> 0% of each run, Pallas kernels for 0% -> 0%
where the time goes in v1:
time: 132 us
  Pallas kernels  117 us (89%)
  local copies, waits for them, and re-layouts  14.1 us (11%)
    pallas_call x1, Pallas kernels, project(): pl.pallas_call(functools.partial(project_kernel, kv, tp), in_specs=[spec(...  54.9 us
    pallas_call x1, Pallas kernels, output(): pl.pallas_call(functools.partial(output_kernel, kv, tp, hd), in_specs=[sp...  52.5 us
    unnamed x40, local copies, waits for them, and re-layouts  13.1 us
    pallas_call x1, Pallas kernels, delta_call(): pl.pallas_call(functools.partial(delta_kernel, prop), grid=(tiles, heads)...  9.48 us

profile of v1, /device:TPU:0, one launch (start us, length us, event | category | flops | bytes accessed | tf_op | source)
XLA Modules:
  0.0 131.8 jit_solution(15686268155829004369)
XLA Ops:
  0.6 0.0 copy-start.1
  0.6 0.0 copy-start
  0.7 0.8 broadcast_in_dim.10.gain
  1.5 0.0 copy-start.2
  1.5 1.6 %copy-done.2 = bf16[2048,256]{1,0:T(8,128)(2,1)S(1)} copy-done((bf16[2048,256]{1,0:T(8,128)(2,1)S(1)}, bf16[2048,256]{1,0:T(8,128)(2,1)}, u32[]{:S(2)}) %copy-start.2) | copy-done | bytes 1048600
  3.1 0.0 copy-start.3
  3.1 1.5 %copy-done.3 = bf16[2048,256]{1,0:T(8,128)(2,1)S(1)} copy-done((bf16[2048,256]{1,0:T(8,128)(2,1)S(1)}, bf16[2048,256]{1,0:T(8,128)(2,1)}, u32[]{:S(2)}) %copy-start.3) | copy-done | bytes 1048600
  4.6 0.0 copy-start.4
  4.6 0.9 copy-done.4
  5.6 0.9 copy-done.5
  6.5 0.9 copy-done.6
  7.5 0.9 copy-done.7
  8.4 0.7 copy-done.8
  9.1 0.7 copy-done.9
  9.8 0.7 copy-done.10
  10.5 0.7 copy-done.11
  11.2 0.7 copy-done.12
  11.9 0.7 copy-done.13
  12.6 0.7 copy-done.14
  13.2 0.7 copy-done.15
  13.9 54.9 %shard_map.203 = (bf16[4,256,256]{2,1,0:T(8,128)(2,1)S(1)}, bf16[4,256,256]{2,1,0:T(8,128)(2,1)S(1)}, bf16[4,64,256]{2,1,0:T(8,128)(2,1)S(1)}, bf16[4,64,256]{2,...) custom-call(bf16[4,64,256]{2,1,0:T(8,128)(2,1)S(1)} %bitcast.29, ...), custom_call_target="tpu_custom_call" | custom-call | flops 2751463424 | bytes 8388608 | tf_op jit(solution)/shard_map/pallas_call | solution.py:311
  68.8 0.0 copy-done.16
  68.8 0.1 copy.24
  68.9 0.0 copy-done.18
  68.9 0.1 broadcast_in_dim.24.hg_ref
  69.0 0.0 copy-done.1
  69.0 0.0 copy-done
  69.0 9.5 %shard_map.204 = (f32[4,64,256]{2,1,0:T(8,128)S(1)}, f32[2,4,256]{2,1,0:T(4,128)S(1)}, f32[256,2,32,128]{3,2,1,0:T(8,128)}) custom-call(bf16[4,256,256]{2,1,0:T(8,128)(2,1)S(1)} %get-tuple-element.11.q_ref, bf16[4,256,256]{2,1,0:T(8,128)(2,1)S(1)} %get-tuple-element.12.k_ref, bf16[4,256,256]{2,1,0:T(8,128)(2,1)S(1)} %bitcast.23, ...), custom_call_target="tpu_custom_call" | custom-call | flops 1073741824 | bytes 16777216 | tf_op jit(solution)/shard_map/pallas_call | solution.py:523
  78.5 0.0 copy-done.17
  78.5 0.1 broadcast_in_dim.25.gain_ref
  78.6 52.5 %shard_map.205 = bf16[4,64,256]{2,1,0:T(8,128)(2,1)S(1)} custom-call(f32[4,64,256]{2,1,0:T(8,128)S(1)} %get-tuple-element.16.m_ref, f32[2,4,256]{2,1,0:T(4,128)S(1)} %get-tuple-element.17.sq_ref, bf16[8,2,64,256]{3,2,1,0:T(8,128)(2,1)S(1)} %get-tuple-element.18.wx_ref, f32[64,256]{1,0:T(8,128)S(1)} %broadcast_in_dim.25.gain_ref), custom_call_target="tpu_custom_call" | custom-call | flops 536870912 | bytes 4194304 | tf_op jit(solution)/shard_map/pallas_call | solution.py:677
  131.1 0.7 copy.26
  (14 shorter events, 0.0 us)
Async XLA Ops:
  0.6 68.4 %copy-start.1 = (bf16[256,4,2,32]{0,3,2,1:T(8,128)(2,1)S(1)}, bf16[256,4,2,32]{0,3,2,1:T(8,128)(2,1)}, u32[]{:S(2)}) copy-start(bf16[256,4,2,32]{0,3,2,1:T(8,128)(2,1)} %param.35) | copy-start | bytes 393220
  0.6 68.4 %copy-start = (f32[256,2,32,128]{3,2,1,0:T(8,128)S(1)}, f32[256,2,32,128]{3,2,1,0:T(8,128)}, u32[]{:S(2)}) copy-start(f32[256,2,32,128]{3,2,1,0:T(8,128)} %s_ref.1) | copy-start | bytes 25165828
  1.5 1.6 %copy-start.2 = (bf16[2048,256]{1,0:T(8,128)(2,1)S(1)}, bf16[2048,256]{1,0:T(8,128)(2,1)}, u32[]{:S(2)}) copy-start(bf16[2048,256]{1,0:T(8,128)(2,1)} %wq.1) | copy-start | bytes 3145732
  3.1 1.5 %copy-start.3 = (bf16[2048,256]{1,0:T(8,128)(2,1)S(1)}, bf16[2048,256]{1,0:T(8,128)(2,1)}, u32[]{:S(2)}) copy-start(bf16[2048,256]{1,0:T(8,128)(2,1)} %wk.1) | copy-start | bytes 3145732
  4.6 0.9 copy-start.4
  5.6 0.9 copy-start.5
  6.5 0.9 copy-start.6
  7.5 0.9 copy-start.7
  8.4 0.7 copy-start.8
  9.1 0.7 copy-start.9
  9.8 0.7 copy-start.10
  10.5 0.7 copy-start.11
  11.2 0.7 copy-start.12
  11.9 0.7 copy-start.13
  12.6 0.7 copy-start.14
  13.2 0.7 copy-start.15
  13.9 54.9 %copy-start.16 = (bf16[256,4,256]{2,1,0:T(4,128)(2,1)S(1)}, bf16[256,4,256]{2,1,0:T(4,128)(2,1)}, u32[]{:S(2)}) copy-start(bf16[256,4,256]{2,1,0:T(4,128)(2,1)} %param.34) | copy-start | bytes 1572868
  13.9 55.0 %copy-start.18 = (bf16[32]{0:T(256)(128)(2,1)S(1)}, bf16[32]{0:T(256)(128)(2,1)}, u32[]{:S(2)}) copy-start(bf16[32]{0:T(256)(128)(2,1)} %param.30) | copy-start | bytes 196
  13.9 64.6 %copy-start.17 = (bf16[64]{0:T(256)(128)(2,1)S(1)}, bf16[64]{0:T(256)(128)(2,1)}, u32[]{:S(2)}) copy-start(bf16[64]{0:T(256)(128)(2,1)} %param.32) | copy-start | bytes 388

commit v2 on v1

--- a/solution.py
+++ b/solution.py
@@ -71,16 +71,10 @@
 
 
 def tree(sizes, order):
-    first, second, third = order
     steps = []
     for offset in offsets(sizes):
-        onward = []
-        if offset[second] == 0 and offset[third] == 0 and offset[first] < sizes[first] - 1:
-            onward.append(first)
-        if offset[third] == 0 and offset[second] < sizes[second] - 1:
-            onward.append(second)
-        if offset[third] < sizes[third] - 1:
-            onward.append(third)
+        reached = max([order.index(d) + 1 for d in range(3) if offset[d]], default=0)
+        onward = [(d, k) for d in order[reached:] for k in range(1, sizes[d])]
         steps.append((offset, onward))
     return steps
 
@@ -94,7 +88,8 @@
     for p in range(pieces):
         for half, (order, sign) in enumerate(orders):
             for offset, onward in tree(sizes, order):
-                events.append((sum(offset) + stagger * p, p, half, offset, onward))
+                level = sum(1 for o in offset if o)
+                events.append((level + stagger * p, p, half, offset, onward))
     return sorted(events, key=lambda e: (e[0], e[1], e[3], e[2]))
 
 
@@ -116,13 +111,14 @@
     def view(self, p, half, offset):
         return self.place(p, half, self.source(half, offset), self.grid.core)
 
-    def copy(self, p, half, offset, dim):
+    def copy(self, p, half, offset, step):
         sign = self.orders[half][1]
-        landed = tuple(o + (1 if d == dim else 0) for d, o in enumerate(offset))
+        dim, count = step
+        landed = tuple(o + (count if d == dim else 0) for d, o in enumerate(offset))
         here = self.view(p, half, offset)
         return remote(
             here, here, self.send.at[p], self.recv.at[p, half, self.slot(landed)],
-            self.grid.device(unit(dim, sign)),
+            self.grid.device(unit(dim, sign * count)),
         )
 
     def share(self, p, half, offset):
@@ -168,23 +164,24 @@
 
 ORDERS = (((0, 1, 2), 1), ((0, 2, 1), -1))
 FLAT = (((0, 1, 2), 1), ((0, 1, 2), -1))
-STAGGER = 2
+STAGGER = 0
+VMEM_ALL = 67043328
 
 
 def project_kernel(
     kv, tp,
-    tok, gain, wq, wk, wv, wz, ws, wd, rate, extra, old_strength, old_decay, accepted, parent, wo,
-    q_out, k_out, v_out, z_out, sc_out, wx_out,
-    xt, wt, gcol, wqk, wout, wx, local, send, recv, both, wsend, wrecv,
+    tok, wq, wk, wv, wz, wo, gain_in, ws_in, wd_in, rate_in, extra_in, strength_in, decay_in,
+    accepted_in, parent_in, old_in,
+    ok_out, q_out, k_out, v_out, z_out, sc_out, wx_out,
+    xt, wt, gcol, wqk, wout, wx, gain, ws, wd, rate, extra, old_strength, old_decay, accepted,
+    parent, old, local, send, recv, both, wsend, wrecv,
 ):
     grid = Grid(kv, tp)
     grid.here()
     pieces, own, seqs = tok.shape
-    width = gain.shape[1]
-    cols = wq.shape[1]
+    width, cols = wq.shape
     small = wv.shape[0]
     heads = rate.shape[1]
-    hd = cols // heads
     part = wout.shape[1] // kv
     half_width = seqs // 2
 
@@ -199,6 +196,13 @@
         pltpu.make_async_copy(wv, wt.at[pl.ds(2 * cols, small)], local.at[4]),
         pltpu.make_async_copy(wz, wt.at[pl.ds(2 * cols + small, small)], local.at[5]),
     ]
+    little = zip(
+        (gain_in, ws_in, wd_in, rate_in, extra_in, strength_in, decay_in, accepted_in, parent_in,
+         old_in),
+        (gain, ws, wd, rate, extra, old_strength, old_decay, accepted, parent, old),
+    )
+    for index, (source, target) in enumerate(little):
+        loads.append(pltpu.make_async_copy(source, target, local.at[6 + index]))
     for load in loads:
         load.start()
 
@@ -209,7 +213,7 @@
     meet(grid, peers)
 
     spread = Spread(
-        grid, grid.sizes, ORDERS, pieces, STAGGER, place, 2, send, recv, both
+        grid, grid.sizes, ORDERS, pieces, 0.5, place, 2, send, recv, both
     )
     loads[0].wait()
     for p in range(pieces):
@@ -224,9 +228,14 @@
         ).start()
     wx[mine, grid.core] = wout[:, pl.ds(pl.multiple_of(mine * part, part), part)]
 
+    for load in loads[6:]:
+        load.wait()
+    gains = gain[...].astype(f32)
     for first in range(0, width, 128):
-        piece = gain[:, first : first + 128].astype(f32)
+        piece = gains[first // 128 : first // 128 + 1, :]
         gcol[first : first + 128, :] = jnp.broadcast_to(piece, (128, 128)).T
+    for p in range(pieces):
+        ok_out[p] = old[:, p, :]
     loads[2].wait()
     loads[3].wait()
     for which in range(2):
@@ -296,25 +305,21 @@
     wx_out[...] = wx[...]
 
 
-def project(kv, tp, width, tokens, gain, wq, wk, wv, wz, ws, wd, rate, extra, strength, decay,
-            accepted, parent, wo):
+def project(kv, tp, *args):
+    tokens, wq, _, wv, _, wo, gain, _, _, rate = args[:10]
     pieces, own, seqs = tokens.shape
-    cols = wq.shape[1]
+    width, cols = wq.shape
     small = wv.shape[0]
     heads = rate.shape[1]
     chips = kv * tp // 2
     part = wo.shape[1] // kv
     rows = 2 * cols + 2 * small + 16 * -(-2 * heads // 16)
-    vmem, anyw = pltpu.VMEM, pl.ANY
-    spec = lambda space: pl.BlockSpec(memory_space=space)
-    grid = Grid(kv, tp)
     return pl.pallas_call(
         functools.partial(project_kernel, kv, tp),
-        in_specs=[spec(s) for s in (
-            anyw, vmem, anyw, anyw, anyw, anyw, vmem, vmem, vmem, vmem, vmem, vmem, vmem, vmem, anyw
-        )],
-        out_specs=[spec(vmem)] * 6,
+        in_specs=[pl.BlockSpec(memory_space=pltpu.HBM)] * len(args),
+        out_specs=[pl.BlockSpec(memory_space=pltpu.VMEM)] * 7,
         out_shape=[
+            jax.ShapeDtypeStruct((pieces, seqs, cols), bf16),
             jax.ShapeDtypeStruct((pieces, seqs, cols), bf16),
             jax.ShapeDtypeStruct((pieces, seqs, cols), bf16),
             jax.ShapeDtypeStruct((pieces, small, seqs), bf16),
@@ -329,7 +334,10 @@
             pltpu.VMEM((2, width, cols), bf16),
             pltpu.VMEM(wo.shape, bf16),
             pltpu.VMEM((kv, 2, wo.shape[0], part), bf16),
-            pltpu.SemaphoreType.DMA((6,)),
+        ]
+        + [pltpu.VMEM(x.shape, x.dtype) for x in args[6:]]
+        + [
+            pltpu.SemaphoreType.DMA((len(args),)),
             pltpu.SemaphoreType.DMA((pieces,)),
             pltpu.SemaphoreType.DMA((pieces, 2, chips)),
             pltpu.SemaphoreType.DMA((2, pieces)),
@@ -337,12 +345,20 @@
             pltpu.SemaphoreType.DMA((kv,)),
         ],
         compiler_params=pltpu.CompilerParams(
-            collective_id=0, has_side_effects=True, vmem_limit_bytes=48 * 1024 * 1024
+            collective_id=0, has_side_effects=True, vmem_limit_bytes=VMEM_ALL
         ),
         cost_estimate=pl.CostEstimate(
             flops=2 * rows * width * pieces * seqs, bytes_accessed=8 << 20, transcendentals=0
         ),
-    )(tokens, gain, wq, wk, wv, wz, ws, wd, rate, extra, strength, decay, accepted, parent, wo)
+    )(*args)
+
+
+def column(row):
+    size = row.shape[1]
+    square = (size, size)
+    chosen = lax.broadcasted_iota(jnp.int32, square, 0) == lax.broadcasted_iota(jnp.int32, square, 1)
+    wide = jnp.broadcast_to(row.astype(f32), square)
+    return jnp.sum(jnp.where(chosen, wide, 0.0), axis=1, keepdims=True)
 
 
 def total(terms):
@@ -482,6 +498,7 @@
             acc = acc - coupling[i, j] * update[j]
         update.append(acc)
 
+    hgain = column(hg_ref[...])
     for p in range(prop):
         i = prop + p
         acc = (eg[i] * inv[positions + p]) * raw[positions + p]
@@ -490,7 +507,7 @@
         sq_ref[0, p : p + 1, :] = jnp.sum(acc * acc, axis=0, keepdims=True)
         gate = z_ref[p].astype(f32)
         gate = gate / (1.0 + jnp.exp(-gate))
-        o_ref[p] = acc * hg_ref[...] * gate
+        o_ref[p] = acc * hgain * gate
 
     weighted = [
         update[j] * (jnp.exp(gam[prop - 1] - gam[j]) * inv[j]) for j in range(prop)
@@ -531,7 +548,7 @@
             turned,
             turned,
             pl.BlockSpec((prop, 1, 8, lanes), lambda t, h: (0, h, 0, t)),
-            pl.BlockSpec((vdim, lanes), lambda t, h: (0, 0)),
+            pl.BlockSpec((1, vdim), lambda t, h: (0, 0)),
             state_spec,
         ],
         out_specs=[
@@ -548,7 +565,7 @@
             pltpu.VMEM((3 * prop, hd, lanes), f32),
             pltpu.VMEM((lanes, lanes), f32),
         ],
-        compiler_params=pltpu.CompilerParams(vmem_limit_bytes=40 * 1024 * 1024),
+        compiler_params=pltpu.CompilerParams(vmem_limit_bytes=VMEM_ALL - (400 << 10)),
         cost_estimate=pl.CostEstimate(
             flops=2 * seqs * heads * vdim * hd * 256,
             bytes_accessed=8 * seqs * heads * vdim * hd,
@@ -577,13 +594,13 @@
     meet(grid, everyone)
 
     row = [(o, f) for o, f in everyone if not o[0] and not o[1]]
-    column = lax.axis_index("tp")
+    lane = lax.axis_index("tp")
     for index, (offset, flip) in enumerate(row):
         remote(
-            sq_ref, squares.at[column], qsend.at[index], qrecv.at[index],
+            sq_ref, squares.at[lane], qsend.at[index], qrecv.at[index],
             grid.device(offset, flip),
         ).start()
-    squares[column] = sq_ref[...]
+    squares[lane] = sq_ref[...]
     for first in range(0, kv):
         piece = wx_ref[first].reshape(2 * chans, feats).astype(f32)
         wt[first] = piece.T.astype(bf16)
@@ -593,7 +610,7 @@
 
     for index, (offset, flip) in enumerate(row):
         remote(
-            sq_ref, squares.at[column], qsend.at[index], qrecv.at[index],
+            sq_ref, squares.at[lane], qsend.at[index], qrecv.at[index],
             grid.device(offset, flip),
         ).wait()
     sizes = (grid.z, grid.y, 1)
@@ -631,7 +648,7 @@
 
     spread.run(finish)
     slot = grid.at[2] * 2 + grid.core
-    me = lax.axis_index("kv") * tp + column
+    me = lax.axis_index("kv") * tp + lane
     for p in range(pieces):
         acc = parts[p, slot]
         for index, offset in enumerate(line):
@@ -657,7 +674,7 @@
         ).wait_recv()
     summed = jnp.sum(sums[...], axis=0)
     final = lax.rsqrt(summed / (kv * tp * own) + epsilon)
-    g = gain_ref[...]
+    g = column(gain_ref[...])
     for p in range(pieces):
         out_ref[p] = (parts[p, slot] * final[p : p + 1, :] * g).astype(bf16)
     rest = sums.at[pl.ds(0, kv * tp - 1)]
@@ -698,7 +715,7 @@
             pltpu.SemaphoreType.DMA((peers,)),
         ],
         compiler_params=pltpu.CompilerParams(
-            collective_id=1, has_side_effects=True, vmem_limit_bytes=32 * 1024 * 1024
+            collective_id=1, has_side_effects=True, vmem_limit_bytes=VMEM_ALL - (200 << 10)
         ),
         cost_estimate=pl.CostEstimate(
             flops=2 * feats * kv * 2 * chans * pieces * seqs, bytes_accessed=4 << 20,
@@ -741,14 +758,15 @@
     def turn(x):
         return jnp.transpose(x, (1, 2, 0))
 
-    q, k, v, z, scal, wx = project(
-        kv, tp, width,
+    old_keys, q, k, v, z, scal, wx = project(
+        kv, tp,
         turn(tokens),
-        input_norm_gain[None, :],
         query_weight,
         key_weight,
         turn(value_weight).reshape(channels, width),
         turn(output_gate_weight).reshape(channels, width),
+        output_weight.reshape(channels, width),
+        input_norm_gain.reshape(width // 128, 128),
         strength_weight.T,
         decay_weight.T,
         head_decay_rate[None, :],
@@ -757,16 +775,13 @@
         turn(previous_log_decay),
         accepted[None, :],
         parent.T,
-        output_weight.reshape(channels, width),
+        previous_keys,
     )
-    old_keys = jnp.transpose(previous_keys, (1, 0, 2))
     old_values = jnp.transpose(previous_values, (1, 2, 3, 0)).reshape(prop, channels, seqs)
-    hgain = jnp.broadcast_to(head_norm_gain.astype(f32)[:, None], (vdim, lanes))
     m, sq, accepted_state = delta_call(
-        lanes, q, k, old_keys, v, old_values, z, scal, hgain, state
+        lanes, q, k, old_keys, v, old_values, z, scal, head_norm_gain[None, :], state
     )
-    ogain = jnp.broadcast_to(output_norm_gain.astype(f32)[:, None], (own, seqs))
-    layer_out = output(kv, tp, hd, own, m, sq, wx, ogain)
+    layer_out = output(kv, tp, hd, own, m, sq, wx, output_norm_gain[None, :])
     return (jnp.transpose(layer_out, (2, 0, 1)), accepted_state)
 
 

time: 132 us -> 89.8 us (0.68)
  Pallas kernels: 117 us -> 87.4 us
  local copies, waits for them, and re-layouts: 14.1 us -> 1.57 us
    pallas_call x1, Pallas kernels: 52.5 us -> 36 us  [output(): pl.pallas_call(functools.partial(output_kernel, kv, tp, hd), in_specs=[sp...]
    pallas_call x1, Pallas kernels: 54.9 us -> 39.7 us  [project(): pl.pallas_call(functools.partial(project_kernel, kv, tp), in_specs=[pl.Bl...]
    unnamed x40 -> x1, local copies, waits for them, and re-layouts: 13.1 us -> 1.57 us
    pallas_call x1, Pallas kernels: 9.48 us -> 11.7 us  [delta_call(): pl.pallas_call(functools.partial(delta_kernel, prop), grid=(tiles, heads)...]
where the time goes in v2:
time: 89.8 us; the launch traced here: 89.6 us
  Pallas kernels  87.4 us (97%)
  local copies, waits for them, and re-layouts  1.57 us (2%)
    pallas_call x1, Pallas kernels, project(): pl.pallas_call(functools.partial(project_kernel, kv, tp), in_specs=[pl.Bl...  39.7 us
    pallas_call x1, Pallas kernels, output(): pl.pallas_call(functools.partial(output_kernel, kv, tp, hd), in_specs=[sp...  36 us
    pallas_call x1, Pallas kernels, delta_call(): pl.pallas_call(functools.partial(delta_kernel, prop), grid=(tiles, heads)...  11.7 us

profile of v2, /device:TPU:0, one launch (start us, length us, event | category | flops | bytes accessed | tf_op | source)
XLA Modules:
  0.0 89.6 jit_solution(15858878212850491715)
XLA Ops:
  0.6 39.7 %shard_map.203 = (bf16[4,256,256]{2,1,0:T(8,128)(2,1)}, bf16[4,256,256]{2,1,0:T(8,128)(2,1)}, bf16[4,256,256]{2,1,0:T(8,128)(2,1)}, bf16[4,64,256]{2,1,0:T(8,128...) custom-call(bf16[4,64,256]{2,1,0:T(8,128)(2,1)} %bitcast.29, ...), custom_call_target="tpu_custom_call" | custom-call | flops 2751463424 | bytes 8388608 | tf_op jit(solution)/shard_map/pallas_call | solution.py:317
  40.4 11.7 %shard_map.204 = (f32[4,64,256]{2,1,0:T(8,128)}, f32[2,4,256]{2,1,0:T(4,128)}, f32[256,2,32,128]{3,2,1,0:T(8,128)}) custom-call(bf16[4,256,256]{2,1,0:T(8,128)(2,1)} %get-tuple-element.12.q_ref, bf16[4,256,256]{2,1,0:T(8,128)(2,1)} %get-tuple-element.13.k_ref, bf16[4,256,256]{2,1,0:T(8,128)(2,1)} %get-tuple-element.14.ok_ref, ...), custom_call_target="tpu_custom_call" | custom-call | flops 1073741824 | bytes 16777216 | tf_op jit(solution)/shard_map/pallas_call | solution.py:540
  52.0 36.0 %shard_map.205 = bf16[4,64,256]{2,1,0:T(8,128)(2,1)} custom-call(f32[4,64,256]{2,1,0:T(8,128)} %get-tuple-element.18.m_ref, f32[2,4,256]{2,1,0:T(4,128)} %get-tuple-element.19.sq_ref, bf16[8,2,64,256]{3,2,1,0:T(8,128)(2,1)} %get-tuple-element.20.wx_ref, bf16[1,64]{1,0:T(2,128)(2,1)} %bitcast.39), custom_call_target="tpu_custom_call" | custom-call | flops 536870912 | bytes 4194304 | tf_op jit(solution)/shard_map/pallas_call | solution.py:694
  88.0 1.6 %copy.23 = bf16[256,4,64]{0,2,1:T(8,128)(2,1)} copy(bf16[256,4,64]{0,2,1:T(8,128)(2,1)} %bitcast.23) | data formatting | bytes 262144

commit v3 on v0

v3 whole, which is shorter than its diff:
```python
import functools

import jax
import jax.numpy as jnp
from jax import lax
from jax.experimental import pallas as pl
from jax.experimental.pallas import tpu as pltpu
from jax.sharding import PartitionSpec as P

epsilon = 1e-06
GROUP = 16
AXES = ("kv", "tp")
MESH = pl.DeviceIdType.MESH
f32, bf16 = jnp.float32, jnp.bfloat16


class Grid:
    def __init__(self, kv, tp):
        self.kv, self.tp = kv, tp
        self.x = tp // 2
        self.y = self.x if kv % self.x == 0 else 1
        self.z = kv // self.y
        self.sizes = (self.z, self.y, self.x)

    def here(self):
        kv, tp = lax.axis_index("kv"), lax.axis_index("tp")
        self.at = (kv // self.y, lax.rem(kv, self.y), tp // 2)
        self.core = lax.rem(tp, 2)

    def shift(self, offset):
        return tuple(lax.rem(a + o % n, n) for a, o, n in zip(self.at, offset, self.sizes))

    def device(self, offset, flip=0):
        z, y, x = self.shift(offset)
        core = 1 - self.core if flip else self.core
        return (z * self.y + y, x * 2 + core)

    def chip(self, offset):
        z, y, x = self.shift(offset)
        return (z * self.y + y) * self.x + x

    def group(self, offset):
        z, y, _ = self.shift(offset)
        return z * self.y + y


def offsets(sizes):
    return [(a, b, c) for a in range(sizes[0]) for b in range(sizes[1]) for c in range(sizes[2])]


def negated(offset, sizes):
    return tuple(-o % n for o, n in zip(offset, sizes))


def meet(grid, peers):
    barrier = pltpu.get_barrier_semaphore()
    for offset, flip in peers:
        pl.semaphore_signal(
            barrier, inc=1, device_id=grid.device(offset, flip), device_id_type=MESH
        )
    pl.semaphore_wait(barrier, len(peers))


def remote(src, dst, send, recv, device):
    return pltpu.make_async_remote_copy(
        src_ref=src, dst_ref=dst, send_sem=send, recv_sem=recv, device_id=device,
        device_id_type=MESH,
    )


def tree(sizes, order):
    steps = []
    for offset in offsets(sizes):
        reached = max([order.index(d) + 1 for d in range(3) if offset[d]], default=0)
        onward = [(d, k) for d in order[reached:] for k in range(1, sizes[d])]
        steps.append((offset, onward))
    return steps


def unit(dim, sign):
    return tuple(sign if d == dim else 0 for d in range(3))


class Spread:
    def __init__(self, grid, sizes, orders, place, send, recv, both):
        self.grid, self.sizes, self.orders = grid, sizes, orders
        self.place, self.send, self.recv, self.both = place, send, recv, both

    def slot(self, offset):
        a, b, c = offset
        return (a * self.sizes[1] + b) * self.sizes[2] + c

    def view(self, u, half, offset):
        sign = self.orders[half][1]
        return self.place(u, half, tuple(-sign * o for o in offset), self.grid.core)

    def pass_on(self, u, half, offset, onward):
        sign = self.orders[half][1]
        here = self.view(u, half, offset)
        for dim, count in onward:
            landed = tuple(o + (count if d == dim else 0) for d, o in enumerate(offset))
            remote(
                here, here, self.send.at[u], self.recv.at[u, half, self.slot(landed)],
                self.grid.device(unit(dim, sign * count)),
            ).start()
        remote(
            here, here, self.both.at[0, u], self.both.at[1, u], self.grid.device((0, 0, 0), 1)
        ).start()

    def begin(self, u):
        for half, (order, _) in enumerate(self.orders):
            for offset, onward in tree(self.sizes, order):
                if not any(offset):
                    self.pass_on(u, half, offset, onward)

    def level(self, u, wanted):
        for half, (order, _) in enumerate(self.orders):
            for offset, onward in tree(self.sizes, order):
                if sum(1 for o in offset if o) != wanted:
                    continue
                here = self.view(u, half, offset)
                remote(
                    here, here, self.send.at[u], self.recv.at[u, half, self.slot(offset)],
                    self.grid.device((0, 0, 0), 1),
                ).wait_recv()
                self.pass_on(u, half, offset, onward)

    def shared(self, u, whole):
        remote(whole, whole, self.both.at[0, u], self.both.at[1, u],
               self.grid.device((0, 0, 0), 1)).wait_recv()

    def sent(self, u, whole, rest):
        far = self.grid.device((0, 0, 0), 1)
        remote(rest, rest, self.send.at[u], self.both.at[1, u], far).wait_send()
        remote(whole, whole, self.both.at[0, u], self.both.at[1, u], far).wait_send()


ORDERS = (((0, 1, 2), 1), ((0, 2, 1), -1))
FLAT = (((0, 1, 2), 1),)
VMEM_ALL = 67043328
LANES = 128


def column(row):
    size = row.shape[1]
    square = (size, size)
    chosen = lax.broadcasted_iota(jnp.int32, square, 0) == lax.broadcasted_iota(jnp.int32, square, 1)
    wide = jnp.broadcast_to(row.astype(f32), square)
    return jnp.sum(jnp.where(chosen, wide, 0.0), axis=1, keepdims=True)


def total(terms):
    terms = list(terms)
    while len(terms) > 1:
        terms = [sum(terms[i : i + 2][1:], terms[i]) for i in range(0, len(terms), 2)]
    return terms[0]


def swap(outer, groups, source, sources, targets):
    shifted = []
    for d in range(groups):
        acc = None
        for a in range(sources):
            t = (a - d) % groups
            if t >= targets:
                continue
            acc = source[a] if acc is None else jnp.where(outer == t, source[a], acc)
        shifted.append(acc if acc is None or d == 0 else pltpu.roll(acc, d * GROUP, 1))
    results = []
    for t in range(targets):
        acc = None
        for a in range(sources):
            piece = shifted[(a - t) % groups]
            acc = piece if acc is None else jnp.where(outer == a, piece, acc)
        results.append(acc)
    return results


def read_state(st, start, h, tiles_of, count):
    vdim, hd = st.shape[2], st.shape[3]
    groups = LANES // GROUP
    lane = lax.broadcasted_iota(jnp.int32, (vdim, LANES), 1)
    inner, outer = lane % GROUP, lane // GROUP
    products = []
    for c in range(groups):
        first = start + c * GROUP
        rows = st[first : first + GROUP, h].reshape(GROUP * vdim, hd).astype(bf16)
        keys = jnp.concatenate(tiles_of(first), axis=0)
        product = lax.dot_general(
            rows, keys, (((1,), (1,)), ((), ())), preferred_element_type=f32
        )
        width = count * GROUP
        chosen = product[:vdim]
        for s in range(1, GROUP):
            chosen = jnp.where(
                inner[:, :width] == s, product[s * vdim : (s + 1) * vdim], chosen
            )
        if width < LANES:
            chosen = jnp.concatenate([chosen, jnp.zeros((vdim, LANES - width), f32)], axis=1)
        products.append(chosen)
    return swap(outer, groups, products, groups, count)


def advance(st, ok, kt, ov, strength, decay, accepted, t, h):
    prop, _, _ = ok.shape
    vdim, hd = st.shape[2], st.shape[3]
    start = t * LANES
    span = slice(start, start + LANES)
    cols = slice(h * hd, (h + 1) * hd)
    groups = LANES // GROUP
    for p in range(prop):
        kt[p] = ok[p, span, cols].astype(f32).T
    inv = [lax.rsqrt(jnp.sum(kt[p] * kt[p], axis=0, keepdims=True) + epsilon) for p in range(prop)]
    count = accepted[:, span]
    live = [jnp.where(count > p, 1.0, 0.0) for p in range(prop)]
    beta = [strength[p, h : h + 1, span] * live[p] for p in range(prop)]
    gam = []
    for p in range(prop):
        step = decay[p, h : h + 1, span] * live[p]
        gam.append(step if p == 0 else gam[-1] + step)
    raw = read_state(
        st, start, h, lambda first: [ok[p, first : first + GROUP, cols] for p in range(prop)], prop
    )
    update = []
    for i in range(prop):
        value = ov[i, h * vdim : (h + 1) * vdim, span].astype(f32)
        acc = beta[i] * value - (beta[i] * jnp.exp(gam[i]) * inv[i]) * raw[i]
        for j in range(i):
            gram = jnp.sum(kt[i] * kt[j], axis=0, keepdims=True) * (inv[i] * inv[j])
            acc = acc - (beta[i] * gram * jnp.exp(jnp.minimum(gam[i] - gam[j], 0.0))) * update[j]
        update.append(acc)
    weighted = [update[j] * (jnp.exp(gam[-1] - gam[j]) * inv[j]) for j in range(prop)]
    lane = lax.broadcasted_iota(jnp.int32, (vdim, LANES), 1)
    inner, outer = lane % GROUP, lane // GROUP
    compact = swap(outer, groups, weighted, prop, groups)
    width = prop * GROUP
    narrow = inner[:, :width]
    fade = jnp.broadcast_to(jnp.exp(gam[-1]), (LANES, LANES)).T
    for c in range(groups):
        first = start + c * GROUP
        keys = jnp.concatenate([ok[p, first : first + GROUP, cols] for p in range(prop)], axis=0)
        piece = compact[c][:, :width]
        left = jnp.concatenate(
            [jnp.where(narrow == s, piece, 0.0) for s in range(GROUP)], axis=0
        ).astype(bf16)
        delta = jnp.dot(left, keys, preferred_element_type=f32)
        for s in range(GROUP):
            seq = c * GROUP + s
            st[start + seq, h] = (
                st[start + seq, h] * fade[seq : seq + 1, :hd] + delta[s * vdim : (s + 1) * vdim]
            )


def propose(st, natural, turned, sc, vz, hgain, m, sq, t, h):
    prop = natural.shape[1]
    vdim, hd = st.shape[2], st.shape[3]
    start = t * LANES
    span = slice(start, start + LANES)
    cols = slice(h * hd, (h + 1) * hd)
    vrows = slice(h * vdim, (h + 1) * vdim)

    def vector(which, p):
        return turned[which, p, cols, span]

    def dot(a, b):
        return jnp.sum(vector(*a) * vector(*b), axis=0, keepdims=True)

    inv_q = [
        lax.rsqrt(dot((0, p), (0, p)) + epsilon) * hd ** (-0.5) for p in range(prop)
    ]
    inv = [lax.rsqrt(dot((1, p), (1, p)) + epsilon) for p in range(prop)]
    beta = [sc[p, h, 0:1, span] for p in range(prop)]
    g = [sc[p, h, 1:2, span] for p in range(prop)]
    parents = [sc[p, h, 2:3, span] for p in range(prop)]
    ancestor = []
    for i in range(prop):
        direct = [jnp.where(parents[i] == float(j), 1.0, 0.0) for j in range(i)]
        row = []
        for j in range(i):
            row.append(total([direct[j]] + [direct[k] * ancestor[k][j] for k in range(j + 1, i)]))
        ancestor.append(row)
    gam = []
    for i in range(prop):
        gam.append(total([g[i]] + [ancestor[i][j] * g[j] for j in range(i)]))
    dec = {
        (i, j): jnp.exp(jnp.minimum(gam[i] - gam[j], 0.0)) * ancestor[i][j]
        for i in range(prop)
        for j in range(i)
    }
    raw = read_state(
        st, start, h,
        lambda first: [
            natural[which, p, first : first + GROUP, cols] for which in (1, 0) for p in range(prop)
        ],
        2 * prop,
    )
    update = []
    for i in range(prop):
        value = vz[0, i, vrows, span].astype(f32)
        acc = beta[i] * value - (beta[i] * jnp.exp(gam[i]) * inv[i]) * raw[i]
        for j in range(i):
            gram = dot((1, i), (1, j)) * (inv[i] * inv[j])
            acc = acc - (beta[i] * gram * dec[i, j]) * update[j]
        update.append(acc)
    for p in range(prop):
        acc = (jnp.exp(gam[p]) * inv_q[p]) * raw[prop + p]
        for j in range(p + 1):
            weight = dot((0, p), (1, j)) * (inv_q[p] * inv[j])
            acc = acc + (weight if j == p else weight * dec[p, j]) * update[j]
        sq[t, h * prop + p : h * prop + p + 1, :] = jnp.sum(acc * acc, axis=0, keepdims=True)
        gate = vz[1, p, vrows, span].astype(f32)
        m[p, vrows, span] = acc * hgain * (gate / (1.0 + jnp.exp(-gate)))


def step_kernel(
    kv, tp,
    tok, wq, wk, wv, wz, wo, state, gain_in, ws_in, wd_in, rate_in, extra_in, strength_in,
    decay_in, accepted_in, parent_in, old_in, ov_in, hgain_in, ogain_in,
    out_ref, st,
    xt, wt, gcol, wqk, wout, wx, wxt, ok, kt, natural, turned, sc, vz, m, sq, squares, xb, parts,
    mine, sums,
    gain, ws, wd, rate, extra, strength, decay, accepted, parent, old, ov, hgain, ogain,
    local, tsem, ssem, send, recv, both, wsend, wrecv, qsend, qrecv, send2, recv2, both2,
    psend, precv, esend, erecv,
):
    grid = Grid(kv, tp)
    grid.here()
    prop, own, seqs = tok.shape
    width, cols = wq.shape
    small = wv.shape[0]
    heads, vdim, hd = st.shape[1:]
    part = wout.shape[1] // kv
    chips = kv * tp // 2
    tiles = seqs // LANES
    pairs = prop // 2
    units = tiles * pairs
    lane = lax.axis_index("tp")
    me = lax.axis_index("kv") * tp + lane
    mine_kv = grid.group((0, 0, 0))
    far = grid.device((0, 0, 0), 1)

    def piece_of(u, half):
        return (u % pairs) * 2 + half, slice((u // pairs) * LANES, (u // pairs + 1) * LANES)

    here = (grid.chip((0, 0, 0)), grid.core)
    token_loads = {}
    for u in range(units):
        for half in range(2):
            p, span = piece_of(u, half)
            token_loads[u, half] = pltpu.make_async_copy(
                tok.at[p, :, span],
                xt.at[u, here[0], here[1], :, pl.ds(half * LANES, LANES)],
                tsem.at[u, half],
            )
            token_loads[u, half].start()
    loads = [
        pltpu.make_async_copy(wo, wout, local.at[0]),
        pltpu.make_async_copy(wq, wqk.at[0], local.at[1]),
        pltpu.make_async_copy(wk, wqk.at[1], local.at[2]),
        pltpu.make_async_copy(wv, wt.at[pl.ds(2 * cols, small)], local.at[3]),
        pltpu.make_async_copy(wz, wt.at[pl.ds(2 * cols + small, small)], local.at[4]),
    ]
    little = zip(
        (gain_in, ws_in, wd_in, rate_in, extra_in, strength_in, decay_in, accepted_in, parent_in,
         old_in, ov_in, hgain_in, ogain_in),
        (gain, ws, wd, rate, extra, strength, decay, accepted, parent, old, ov, hgain, ogain),
    )
    for index, (source, target) in enumerate(little):
        loads.append(pltpu.make_async_copy(source, target, local.at[5 + index]))
    for load in loads:
        load.start()
    state_loads = {}
    for t in range(tiles):
        for h in range(heads):
            state_loads[t, h] = pltpu.make_async_copy(
                state.at[pl.ds(t * LANES, LANES), h], st.at[pl.ds(t * LANES, LANES), h],
                ssem.at[t, h],
            )
            state_loads[t, h].start()

    everyone = [(o, f) for o in offsets(grid.sizes) for f in (0, 1)]
    everyone = [e for e in everyone if any(e[0]) or e[1]]
    row = [(o, f) for o, f in everyone if not o[0] and not o[1]]
    plane = [o for o in offsets((grid.z, grid.y, 1)) if any(o)]
    line = [(0, 0, c) for c in range(1, grid.x)]
    meet(grid, everyone)

    tokens = Spread(
        grid, grid.sizes, ORDERS,
        lambda u, half, offset, core: xt.at[
            u, grid.chip(offset), core, :, pl.ds(half * LANES, LANES)
        ],
        send, recv, both,
    )
    blend = Spread(
        grid, (grid.z, grid.y, 1), FLAT,
        lambda u, half, offset, core: xb.at[u, grid.group(offset), core],
        send2, recv2, both2,
    )

    def weights_in():
        for load in loads:
            load.wait()
        gains = gain[...].astype(f32)
        for first in range(0, width, 128):
            piece = gains[first // 128 : first // 128 + 1, :]
            gcol[first : first + 128, :] = jnp.broadcast_to(piece, (128, 128)).T
        for which in range(2):
            for first in range(0, width, 256):
                piece = wqk[which, first : first + 256, :].astype(f32)
                wt[which * cols : (which + 1) * cols, first : first + 256] = piece.T.astype(bf16)
        tail = wt.shape[0] - 2 * cols - 2 * small
        rows = [ws[...].astype(f32), wd[...].astype(f32)]
        rows.append(jnp.zeros((tail - 2 * heads, width), f32))
        wt[2 * cols + 2 * small :, :] = jnp.concatenate(rows, axis=0).astype(bf16)
        for p in range(prop):
            ok[p] = old[:, p, :]

    def take_up(t, h):
        state_loads[t, h].wait()
        advance(st, ok, kt, ov, strength, decay, accepted, t, h)

    def weights_out():
        for index, offset in enumerate(plane):
            start = pl.multiple_of(grid.group(offset) * part, part)
            remote(
                wout.at[:, pl.ds(start, part)], wx.at[mine_kv, grid.core],
                wsend.at[0], wrecv.at[index], grid.device(offset),
            ).start()
        wx[mine_kv, grid.core] = wout[:, pl.ds(pl.multiple_of(mine_kv * part, part), part)]
        remote(
            wout.at[:, pl.ds(pl.multiple_of(mine_kv * part, part), part)],
            wx.at[mine_kv, grid.core], wsend.at[1], wrecv.at[len(plane)], far,
        ).start()

    def weights_over():
        for index, offset in enumerate(plane):
            view = wx.at[grid.group(negated(offset, grid.sizes)), grid.core]
            remote(view, view, wsend.at[0], wrecv.at[index], far).wait_recv()
            remote(view, view, wsend.at[1], wrecv.at[len(plane)], far).start()

    def weights_turn():
        other = wx.at[:, 1 - grid.core]
        remote(other, other, wsend.at[1], wrecv.at[len(plane)], far).wait_recv()
        for g in range(kv):
            piece = wx[g].reshape(2 * small, part).astype(f32)
            wxt[g] = piece.T.astype(bf16)

    def finish(u):
        tokens.shared(u, xt.at[u, :, 1 - grid.core])
        x = xt[u].reshape(width, 2 * LANES).astype(f32)
        square = jnp.sum(x * x, axis=0, keepdims=True)
        scale = lax.rsqrt(square / width + epsilon)
        g = jnp.concatenate([gcol[...]] * 2, axis=1)
        normed = (x * scale * g).astype(bf16)
        out = jnp.dot(wt[...], normed, preferred_element_type=f32)
        for half in range(2):
            p, span = piece_of(u, half)
            lanes = slice(half * LANES, (half + 1) * LANES)
            for which in range(2):
                block = out[which * cols : (which + 1) * cols, lanes].astype(bf16).astype(f32)
                turned[which, p, :, span] = block
                natural[which, p, span, :] = block.T.astype(bf16)
                first = 2 * cols + which * small
                vz[which, p, :, span] = out[first : first + small, lanes].astype(bf16)
            side = out[2 * cols + 2 * small :, lanes]
            for h in range(heads):
                pre = side[heads + h : heads + h + 1]
                beta = 1.0 / (1.0 + jnp.exp(-side[h : h + 1]))
                soft = jnp.maximum(pre, 0.0) + jnp.log1p(jnp.exp(-jnp.abs(pre)))
                g_new = -rate[0:1, h : h + 1] * soft + extra[p, h : h + 1, span]
                sc[p, h, 0:1, span] = beta
                sc[p, h, 1:2, span] = g_new
                sc[p, h, 2:3, span] = parent[p : p + 1, span].astype(f32)

    def read_out(t):
        gains = column(hgain[...])
        for h in range(heads):
            propose(st, natural, turned, sc, vz, gains, m, sq, t, h)
        for index, (offset, flip) in enumerate(row):
            remote(
                sq.at[t], squares.at[t, lane], qsend.at[t, index], qrecv.at[t, index],
                grid.device(offset, flip),
            ).start()
        squares[t, lane] = sq[t]

    def blend_out(t):
        for index, (offset, flip) in enumerate(row):
            remote(
                sq.at[t], squares.at[t, lane], qsend.at[t, index], qrecv.at[t, index],
                grid.device(offset, flip),
            ).wait()
        everything = total([squares[t, i] for i in range(tp)])
        scale = lax.rsqrt(everything / hd + epsilon)
        for u in range(t * pairs, (t + 1) * pairs):
            for half in range(2):
                p, span = piece_of(u, half)
                scaled = [
                    m[p, h * vdim : (h + 1) * vdim, span]
                    * scale[h * prop + p : h * prop + p + 1, :]
                    for h in range(heads)
                ]
                xb[u, mine_kv, grid.core, :, half * LANES : (half + 1) * LANES] = (
                    jnp.concatenate(scaled, axis=0).astype(bf16)
                )
            blend.begin(u)

    def exchange(u, index, offset):
        target = grid.shift(offset)[2] * 2 + grid.core
        return remote(
            parts.at[u, target], mine.at[u, index], psend.at[u, index], precv.at[u, index],
            grid.device(offset),
        )

    def multiply(u):
        blend.shared(u, xb.at[u, :, 1 - grid.core])
        out = None
        for g in range(kv):
            term = jnp.dot(
                wxt[g], xb[u, g].reshape(2 * small, 2 * LANES), preferred_element_type=f32
            )
            out = term if out is None else out + term
        parts[u] = out.reshape(part // own, own, 2 * LANES)
        for index, offset in enumerate(line):
            exchange(u, index, offset).start()

    slot = grid.at[2] * 2 + grid.core

    def square_out(t):
        for u in range(t * pairs, (t + 1) * pairs):
            acc = parts[u, slot]
            for index, offset in enumerate(line):
                exchange(u, index, offset).wait()
                acc = acc + mine[u, index]
            parts[u, slot] = acc
            pp = u - t * pairs
            sums[t, me, pp : pp + 1, :] = jnp.sum(acc * acc, axis=0, keepdims=True)
        for index, (offset, flip) in enumerate(everyone):
            remote(
                sums.at[t, me], sums.at[t, me], esend.at[t], erecv.at[t, index],
                grid.device(offset, flip),
            ).start()

    def end(t):
        for index, (offset, flip) in enumerate(everyone):
            kv_from, tp_from = grid.device(negated(offset, grid.sizes), flip)
            view = sums.at[t, kv_from * tp + tp_from]
            remote(view, view, esend.at[t], erecv.at[t, index], far).wait_recv()
        final = lax.rsqrt(jnp.sum(sums[t], axis=0) / width + epsilon)
        g = column(ogain[...])
        for u in range(t * pairs, (t + 1) * pairs):
            pp = u - t * pairs
            for half in range(2):
                p, span = piece_of(u, half)
                lanes = slice(half * LANES, (half + 1) * LANES)
                out_ref[p, :, span] = (
                    parts[u, slot][:, lanes] * final[pp : pp + 1, lanes] * g
                ).astype(bf16)

    for u in range(units):
        for half in range(2):
            token_loads[u, half].wait()
        tokens.begin(u)

    tasks = [(0.5, weights_in), (2.7, weights_out), (WEIGHTS_OVER, weights_over)]
    for u in range(units):
        for level in (1, 2, 3):
            tasks.append((level + 0.5 * u, functools.partial(tokens.level, u, level)))
        tasks.append((3.001 + 0.5 * u, functools.partial(finish, u)))
    places = [(t, h) for t in range(tiles) for h in range(heads)]
    for index, (t, h) in enumerate(places):
        tasks.append((TAKE_UP + 0.4 * index * 4 / len(places), functools.partial(take_up, t, h)))
    last = 3.0 + 0.5 * (units - 1)
    tasks.append((last + 0.02, weights_turn))
    for t in range(tiles):
        ready = 3.0 + 0.5 * ((t + 1) * pairs - 1)
        tasks.append((ready + 0.01, functools.partial(read_out, t)))
        sends = ready + 0.5005 if t < tiles - 1 else last + 0.03
        tasks.append((sends, functools.partial(blend_out, t)))
        for u in range(t * pairs, (t + 1) * pairs):
            first = last + 0.021 + 0.1 * t
            late = last + 0.04 + 0.1 * t
            tasks.append((first + 0.0001 * u, functools.partial(blend.level, u, 1)))
            tasks.append((late + 0.002 * u, functools.partial(blend.level, u, 2)))
            tasks.append((late + 0.002 * u + 0.001, functools.partial(multiply, u)))
        tasks.append((last + 0.13 + 0.1 * t, functools.partial(square_out, t)))
        tasks.append((last + 1.0 + t, functools.partial(end, t)))
    for _, task in sorted(tasks, key=lambda entry: entry[0]):
        task()

    rest = wx.at[pl.ds(0, kv - 1), 0]
    remote(rest, rest, wsend.at[0], wrecv.at[0], far).wait_send()
    whole = wx.at[:, 0]
    remote(whole, whole, wsend.at[1], wrecv.at[0], far).wait_send()
    for u in range(units):
        tokens.sent(u, xt.at[u, :, 0], xt.at[u, pl.ds(0, chips - 1), 0])
        blend.sent(u, xb.at[u, :, 0], xb.at[u, pl.ds(0, kv - 1), 0])
    for t in range(tiles):
        rest = sums.at[t, pl.ds(0, kv * tp - 1)]
        remote(rest, rest, esend.at[t], erecv.at[t, 0], far).wait_send()


WEIGHTS_OVER = 3.52
TAKE_UP = 1.6


def step(kv, tp, *args):
    tokens, wq, _, wv, _, wo, state = args[:7]
    prop, own, seqs = tokens.shape
    width, cols = wq.shape
    small = wv.shape[0]
    heads, vdim, hd = state.shape[1:]
    chips = kv * tp // 2
    part = wo.shape[1] // kv
    rows = 2 * cols + 2 * small + 16 * -(-2 * heads // 16)
    tiles = seqs // LANES
    units = tiles * (prop // 2)
    others = max(tp // 2 - 1, 1)
    vmem, dma = pltpu.VMEM, pltpu.SemaphoreType.DMA
    return pl.pallas_call(
        functools.partial(step_kernel, kv, tp),
        in_specs=[pl.BlockSpec(memory_space=pl.ANY)] * len(args),
        out_specs=[pl.BlockSpec(memory_space=pltpu.VMEM)] * 2,
        out_shape=[vmem((prop, own, seqs), bf16), vmem(state.shape, f32)],
        scratch_shapes=[
            vmem((units, chips, 2, own, 2 * LANES), bf16),
            vmem((rows, width), bf16),
            vmem((width, 128), f32),
            vmem((2, width, cols), bf16),
            vmem(wo.shape, bf16),
            vmem((kv, 2, small, part), bf16),
            vmem((kv, part, 2 * small), bf16),
            vmem((prop, seqs, cols), bf16),
            vmem((prop, hd, LANES), f32),
            vmem((2, prop, seqs, cols), bf16),
            vmem((2, prop, cols, seqs), f32),
            vmem((prop, heads, 8, seqs), f32),
            vmem((2, prop, small, seqs), bf16),
            vmem((prop, small, seqs), f32),
            vmem((tiles, heads * prop, LANES), f32),
            vmem((tiles, tp, heads * prop, LANES), f32),
            vmem((units, kv, 2, small, 2 * LANES), bf16),
            vmem((units, part // own, own, 2 * LANES), f32),
            vmem((units, others, own, 2 * LANES), f32),
            vmem((tiles, kv * tp, prop // 2, 2 * LANES), f32),
        ]
        + [vmem(x.shape, x.dtype) for x in args[7:]]
        + [
            dma((len(args) - 2,)),
            dma((units, 2)),
            dma((tiles, heads)),
            dma((units,)),
            dma((units, 2, chips)),
            dma((2, units)),
            dma((2,)),
            dma((kv,)),
            dma((tiles, tp)),
            dma((tiles, tp)),
            dma((units,)),
            dma((units, 1, kv)),
            dma((2, units)),
            dma((units, others)),
            dma((units, others)),
            dma((tiles,)),
            dma((tiles, kv * tp)),
        ],
        compiler_params=pltpu.CompilerParams(
            collective_id=0, has_side_effects=True, vmem_limit_bytes=VMEM_ALL - (9 << 20)
        ),
        cost_estimate=pl.CostEstimate(
            flops=2 * rows * width * prop * seqs, bytes_accessed=16 << 20, transcendentals=0
        ),
    )(*[x if x.size == 1 else pltpu.with_memory_space_constraint(x, pltpu.HBM) for x in args])


def on_device(
    kv,
    tp,
    tokens,
    input_norm_gain,
    query_weight,
    key_weight,
    value_weight,
    output_gate_weight,
    strength_weight,
    decay_weight,
    head_decay_rate,
    proposal_log_decay,
    head_norm_gain,
    output_weight,
    output_norm_gain,
    state,
    previous_keys,
    previous_values,
    previous_log_decay,
    previous_strengths,
    accepted,
    parent,
):
    seqs, heads, vdim, hd = state.shape
    prop = parent.shape[1]
    width = input_norm_gain.shape[0]
    channels = heads * vdim

    def turn(x):
        return jnp.transpose(x, (1, 2, 0))

    layer_out, accepted_state = step(
        kv, tp,
        turn(tokens),
        query_weight,
        key_weight,
        turn(value_weight).reshape(channels, width),
        turn(output_gate_weight).reshape(channels, width),
        output_weight.reshape(channels, width),
        state,
        input_norm_gain.reshape(width // 128, 128),
        strength_weight.T,
        decay_weight.T,
        head_decay_rate[None, :],
        turn(proposal_log_decay),
        turn(previous_strengths),
        turn(previous_log_decay),
        accepted[None, :],
        parent.T,
        previous_keys,
        jnp.transpose(previous_values, (1, 2, 3, 0)).reshape(prop, channels, seqs),
        head_norm_gain[None, :],
        output_norm_gain[None, :],
    )
    return (jnp.transpose(layer_out, (2, 0, 1)), accepted_state)


def solution(mesh):
    placed = (
        P(None, None, AXES),
        P(),
        P(None, "kv"),
        P(None, "kv"),
        P(None, "kv", "tp"),
        P(None, "kv", "tp"),
        P(None, "kv"),
        P(None, "kv"),
        P("kv"),
        P(None, None, "kv"),
        P("tp"),
        P("kv", "tp", None),
        P(AXES),
        P(None, "kv", "tp", None),
        P(None, None, "kv"),
        P(None, None, "kv", "tp"),
        P(None, None, "kv"),
        P(None, None, "kv"),
        P(),
        P(),
    )
    return jax.shard_map(
        functools.partial(on_device, mesh.shape["kv"], mesh.shape["tp"]),
        mesh=mesh,
        in_specs=placed,
        out_specs=(P(None, None, AXES), P(None, "kv", "tp", None)),
        check_vma=False,
    )
```

time: 218 us -> 72.3 us (0.33)
  waiting for transfers between devices: 108 us -> 0 us
  Pallas kernels: 9.3 us -> 67.5 us
  blocking collectives: 44.4 us -> 0 us
  between operations: 14.5 us -> 0.65 us
  matrix products: 11.3 us -> 0 us
  other arithmetic: 10.6 us -> 0 us
  local copies, waits for them, and re-layouts: 13.8 us -> 4.05 us
  starting transfers between devices: 4.49 us -> 0 us
    pallas_call x1, Pallas kernels: 9.3 us -> 67.5 us  [step(): pl.pallas_call(functools.partial(step_kernel, kv, tp), in_specs=[pl.Block...]
    all_gather x1 -> x0, waiting for transfers between devices: 54.5 us -> none  [on_device(): gathered = lax.all_gather(order(tokens), AXES, axis=1, tiled=True)]
    psum x2 -> x0, blocking collectives: 44.4 us -> none  [the longest x1 37.5 us: on_device(): sumsq = lax.psum(jnp.sum(share * share, axis=0), AXES)]
    ppermute x2 -> x0, waiting for transfers between devices: 28.1 us -> none  [the longest x1 24.7 us: scattered_sum(): other = lax.ppermute(other, 'tp', across)]
    all_to_all x1 -> x0, waiting for transfers between devices: 25.5 us -> none  [scattered_sum(): parts = lax.all_to_all(summed, 'kv', 0, 0, tiled=True)]
    dot_general x5 -> x0, matrix products: 11.3 us -> none  [the longest x1 4.09 us: on_device(): keys = jnp.dot(normed, key_weight, preferred_element_type=f32).astype(bf16)]
    reshape x19 -> x0, local copies, waits for them, and re-layouts: 6.51 us -> none  [the longest x11 3.19 us: order(): x = x.reshape((tiles, lanes, prop) + tail)]
    convert_element_type x8 -> x0, other arithmetic: 5.55 us -> none  [the longest x1 2.65 us: scattered_sum(): summed = (mine.astype(f32) + other.astype(f32)).astype(bf16)]
  transfers between devices with their start and end apart: 4 -> 0, of which waited for: 4 -> 0; matrix products, arithmetic and copies ran while one was open for 6% -> 0% of each run, Pallas kernels for 0% -> 0%
where the time goes in v3:
time: 72.3 us; the launch traced here: 72.2 us
  Pallas kernels  67.5 us (93%)
  local copies, waits for them, and re-layouts  4.05 us (6%)
    pallas_call x1, Pallas kernels, step(): pl.pallas_call(functools.partial(step_kernel, kv, tp), in_specs=[pl.Block...  67.5 us
    unnamed x2, local copies, waits for them, and re-layouts  4.05 us

profile of v3, /device:TPU:0, one launch (start us, length us, event | category | flops | bytes accessed | tf_op | source)
XLA Modules:
  0.0 72.2 jit_solution(11540444437939048598)
XLA Ops:
  0.6 67.5 %shard_map.203 = (bf16[4,64,256]{2,1,0:T(8,128)(2,1)S(1)}, f32[256,2,32,128]{3,2,1,0:T(8,128)S(1)}) custom-call(bf16[4,64,256]{2,1,0:T(8,128)(2,1)} %bitcast.27, bf16[2048,256]{1,0:T(8,128)(2,1)} %wq.1, bf16[2048,256]{1,0:T(8,128)(2,1)} %wk.1, bf16[64,2048]{1,0:T(8,128)(2,1)} %bitcast.24, bf16[64,2048]{1,0:T(8,128)(2,1)} %bitcast.25, ...), custom_call_target="tpu_custom_call" | custom-call | flops 2751463424 | bytes 16777216 | tf_op jit(solution)/shard_map/pallas_call | solution.py:620
  68.1 0.7 copy.24
  68.8 3.4 %copy.25 = f32[256,2,32,128]{3,2,1,0:T(8,128)} copy(f32[256,2,32,128]{3,2,1,0:T(8,128)S(1)} %get-tuple-element.7) | data formatting | bytes 16777216

commit v4 on v3

--- a/solution.py
+++ b/solution.py
@@ -318,7 +318,7 @@
     decay_in, accepted_in, parent_in, old_in, ov_in, hgain_in, ogain_in,
     out_ref, st,
     xt, wt, gcol, wqk, wout, wx, wxt, ok, kt, natural, turned, sc, vz, m, sq, squares, xb, parts,
-    mine, sums,
+    leave, mine, sums,
     gain, ws, wd, rate, extra, strength, decay, accepted, parent, old, ov, hgain, ogain,
     local, tsem, ssem, send, recv, both, wsend, wrecv, qsend, qrecv, send2, recv2, both2,
     psend, precv, esend, erecv,
@@ -383,7 +383,8 @@
     row = [(o, f) for o, f in everyone if not o[0] and not o[1]]
     plane = [o for o in offsets((grid.z, grid.y, 1)) if any(o)]
     line = [(0, 0, c) for c in range(1, grid.x)]
-    meet(grid, everyone)
+    near = [(unit(d, k), 0) for d in range(3) for k in range(1, grid.sizes[d])]
+    meet(grid, near + [((0, 0, 0), 1)])
 
     tokens = Spread(
         grid, grid.sizes, ORDERS,
@@ -508,7 +509,7 @@
     def exchange(u, index, offset):
         target = grid.shift(offset)[2] * 2 + grid.core
         return remote(
-            parts.at[u, target], mine.at[u, index], psend.at[u, index], precv.at[u, index],
+            leave.at[u, target], mine.at[u, index], psend.at[u, index], precv.at[u, index],
             grid.device(offset),
         )
 
@@ -521,6 +522,7 @@
             )
             out = term if out is None else out + term
         parts[u] = out.reshape(part // own, own, 2 * LANES)
+        leave[u] = parts[u].astype(bf16)
         for index, offset in enumerate(line):
             exchange(u, index, offset).start()
 
@@ -531,7 +533,7 @@
             acc = parts[u, slot]
             for index, offset in enumerate(line):
                 exchange(u, index, offset).wait()
-                acc = acc + mine[u, index]
+                acc = acc + mine[u, index].astype(f32)
             parts[u, slot] = acc
             pp = u - t * pairs
             sums[t, me, pp : pp + 1, :] = jnp.sum(acc * acc, axis=0, keepdims=True)
@@ -562,29 +564,25 @@
             token_loads[u, half].wait()
         tokens.begin(u)
 
-    tasks = [(0.5, weights_in), (2.7, weights_out), (WEIGHTS_OVER, weights_over)]
-    for u in range(units):
-        for level in (1, 2, 3):
-            tasks.append((level + 0.5 * u, functools.partial(tokens.level, u, level)))
-        tasks.append((3.001 + 0.5 * u, functools.partial(finish, u)))
+    tasks = [(0.5, weights_in), (W_OUT, weights_out), (W_OVER, weights_over), (W_TURN, weights_turn)]
     places = [(t, h) for t in range(tiles) for h in range(heads)]
     for index, (t, h) in enumerate(places):
-        tasks.append((TAKE_UP + 0.4 * index * 4 / len(places), functools.partial(take_up, t, h)))
-    last = 3.0 + 0.5 * (units - 1)
-    tasks.append((last + 0.02, weights_turn))
+        tasks.append((TAKE_UP[min(index, len(TAKE_UP) - 1)], functools.partial(take_up, t, h)))
     for t in range(tiles):
-        ready = 3.0 + 0.5 * ((t + 1) * pairs - 1)
-        tasks.append((ready + 0.01, functools.partial(read_out, t)))
-        sends = ready + 0.5005 if t < tiles - 1 else last + 0.03
-        tasks.append((sends, functools.partial(blend_out, t)))
-        for u in range(t * pairs, (t + 1) * pairs):
-            first = last + 0.021 + 0.1 * t
-            late = last + 0.04 + 0.1 * t
-            tasks.append((first + 0.0001 * u, functools.partial(blend.level, u, 1)))
-            tasks.append((late + 0.002 * u, functools.partial(blend.level, u, 2)))
-            tasks.append((late + 0.002 * u + 0.001, functools.partial(multiply, u)))
-        tasks.append((last + 0.13 + 0.1 * t, functools.partial(square_out, t)))
-        tasks.append((last + 1.0 + t, functools.partial(end, t)))
+        when = TIMES[min(t, 1)] + (t // 2,)
+        lift = when[-1] * 10.0
+        for pp in range(pairs):
+            u = t * pairs + pp
+            for level in (1, 2, 3):
+                tasks.append((lift + when[0][level - 1][pp], functools.partial(tokens.level, u, level)))
+            tasks.append((lift + when[0][2][pp] + 0.001, functools.partial(finish, u)))
+            for level in (1, 2):
+                tasks.append((lift + when[3][level - 1][pp], functools.partial(blend.level, u, level)))
+            tasks.append((lift + when[3][1][pp] + 0.001, functools.partial(multiply, u)))
+        tasks.append((lift + when[1], functools.partial(read_out, t)))
+        tasks.append((lift + when[2], functools.partial(blend_out, t)))
+        tasks.append((lift + when[4], functools.partial(square_out, t)))
+        tasks.append((lift + when[5], functools.partial(end, t)))
     for _, task in sorted(tasks, key=lambda entry: entry[0]):
         task()
 
@@ -600,8 +598,12 @@
         remote(rest, rest, esend.at[t], erecv.at[t, 0], far).wait_send()
 
 
-WEIGHTS_OVER = 3.52
-TAKE_UP = 1.6
+TIMES = (
+    (((1.0, 1.5), (2.0, 2.5), (3.0, 3.5)), 3.51, 4.0005, ((4.521, 4.522), (4.54, 4.542)), 4.63, 8.0),
+    (((2.0, 2.5), (3.0, 3.5), (4.0, 4.5)), 4.51, 4.53, ((4.621, 4.622), (4.644, 4.646)), 4.73, 8.1),
+)
+TAKE_UP = (1.6, 2.01, 2.4, 2.8)
+W_OUT, W_OVER, W_TURN = 3.002, 4.531, 4.5315
 
 
 def step(kv, tp, *args):
@@ -641,7 +643,8 @@
             vmem((tiles, tp, heads * prop, LANES), f32),
             vmem((units, kv, 2, small, 2 * LANES), bf16),
             vmem((units, part // own, own, 2 * LANES), f32),
-            vmem((units, others, own, 2 * LANES), f32),
+            vmem((units, part // own, own, 2 * LANES), bf16),
+            vmem((units, others, own, 2 * LANES), bf16),
             vmem((tiles, kv * tp, prop // 2, 2 * LANES), f32),
         ]
         + [vmem(x.shape, x.dtype) for x in args[7:]]

time: 72.3 us -> 68.3 us (0.945)
  Pallas kernels: 67.5 us -> 63.4 us
    pallas_call x1, Pallas kernels: 67.5 us -> 63.4 us  [step(): pl.pallas_call(functools.partial(step_kernel, kv, tp), in_specs=[pl.Block...]
where the time goes in v4:
time: 68.3 us; the launch traced here: 68.1 us
  Pallas kernels  63.4 us (93%)
  local copies, waits for them, and re-layouts  4.05 us (6%)
    pallas_call x1, Pallas kernels, step(): pl.pallas_call(functools.partial(step_kernel, kv, tp), in_specs=[pl.Block...  63.4 us
    unnamed x2, local copies, waits for them, and re-layouts  4.05 us

profile of v4, /device:TPU:0, one launch (start us, length us, event | category | flops | bytes accessed | tf_op | source)
XLA Modules:
  0.0 68.1 jit_solution(5110676915888561234)
XLA Ops:
  0.6 63.4 %shard_map.203 = (bf16[4,64,256]{2,1,0:T(8,128)(2,1)S(1)}, f32[256,2,32,128]{3,2,1,0:T(8,128)S(1)}) custom-call(bf16[4,64,256]{2,1,0:T(8,128)(2,1)} %bitcast.27, bf16[2048,256]{1,0:T(8,128)(2,1)} %wq.1, bf16[2048,256]{1,0:T(8,128)(2,1)} %wk.1, bf16[64,2048]{1,0:T(8,128)(2,1)} %bitcast.24, bf16[64,2048]{1,0:T(8,128)(2,1)} %bitcast.25, ...), custom_call_target="tpu_custom_call" | custom-call | flops 2751463424 | bytes 16777216 | tf_op jit(solution)/shard_map/pallas_call | solution.py:622
  64.1 0.7 copy.24
  64.7 3.4 %copy.25 = f32[256,2,32,128]{3,2,1,0:T(8,128)} copy(f32[256,2,32,128]{3,2,1,0:T(8,128)S(1)} %get-tuple-element.7) | data formatting | bytes 16777216
